TPU v7x, 32 devices: a whole 2x2x4 slice. The times are simulated.
32 devices in a mesh: sp: 8 (over z, y), tp: 4 (over x, core).
Axes of the slice: x: 2, y: 2, z: 4, core: 2. Of those that a mesh axis runs over, the one named last changes fastest.
Arguments:
- proj_value: bfloat16 [4096, 2016], P('sp', 'tp'), may hold values from -6 to 6
- proj_gate: bfloat16 [4096, 2016], P('sp', 'tp'), may hold values from -8 to 8
- conv_saved: bfloat16 [4096, 2016], P('sp', 'tp'), may hold values from -12 to 12
- conv_taps: bfloat16 [31, 2016], P(None, 'tp'), may hold values from -1 to 1
- norm_gain: bfloat16 [2016], P('tp'), may hold values from 0.099609375 to 1.8984375
- out_weight: bfloat16 [2016, 2016], P('tp'), may hold values from -0.125 to 0.125
- cotangent: bfloat16 [4096, 2016], P('sp'), may hold values from -6 to 6
Outputs:
- grad_value: bfloat16 [4096, 2016], P('sp', 'tp')
- grad_gate: bfloat16 [4096, 2016], P('sp', 'tp')
- grad_out_weight: float32 [2016, 2016], P('tp', 'sp')
- grad_taps: float32 [31, 2016], P(None, 'tp')
All inputs are finite; a program needn't handle non-finite values.
Results may differ from a plain program's by a relative error of at most 0.003.
Values sent between devices are 32-bit elements; how exact they have to be, the bound alone decides.
A program may use at most 64 MiB of HBM per device.

v0:
```python
import functools
import math

import jax
import jax.numpy as jnp
from jax import lax
from jax.experimental import pallas as pl
from jax.experimental.pallas import tpu as pltpu
from jax.sharding import PartitionSpec as P

norm_eps = 1e-05
MESH = pl.DeviceIdType.MESH
f32 = jnp.float32


def line_order(length):
    rows = []
    for place in range(length):
        side = 1 if 2 * place >= length else -1
        rows.append(sorted(range(length), key=lambda d: (-abs(d - place), -side * (d - place))))
    return rows


def low_rows(ch):
    return max(ch // 7 // 8 * 8, 8)


def lookup(table, place):
    value = table[0]
    for i in range(1, len(table)):
        value = jnp.where(place == i, table[i], value)
    return value


def finish(v_in, g_in, w_in, t_in, v_out, g_out, w_out, t_out, v_b, g_b, w_b, t_b, ss):
    trips = [(v_in, v_b, v_out), (g_in, g_b, g_out), (w_in, w_b, w_out), (t_in, t_b, t_out)]
    inward = [pltpu.make_async_copy(a, b, ss.at[i]) for i, (a, b, _) in enumerate(trips)]
    outward = [pltpu.make_async_copy(b, c, ss.at[4 + i]) for i, (_, b, c) in enumerate(trips)]
    for c in inward:
        c.start()
    for a, b in zip(inward, outward):
        a.wait()
        b.start()
    for b in outward:
        b.wait()


def kernel(
    n_sp, n_tp, fold, pv_h, pg_h, conv, taps, gain, weight_h, cot_h,
    out_v, out_g, out_w, out_t,
    pv, pg, weight, cot, in_sems, gain_c, gated_s, d_glu_s, act_t, d_act, ext, shifted, cols, cols2, term, got_y, got_r, got_l, low_r, low_l, low_y,
    stat, stat_in, mom, mom_in, grad_acc, g_own, g_mid, g_in, g_yin, taps_b,
    stat_ss, stat_rs, mom_ss, mom_rs, y_ss, y_rs, r_ss, r_rs, l_ss, l_rs,
    lr_ss, lr_rs, ll_ss, ll_rs, ly_ss, ly_rs,
    halo_ss, halo_rs, gz_ss, gz_rs, gy_ss, gy_rs,
):
    s = lax.axis_index("sp")
    t = lax.axis_index("tp")
    n_z = n_sp // fold
    z = s // fold
    y = s % fold
    other_y = 1 - y
    width, rows = cot.shape
    ch = conv.shape[0]
    part = out_w.shape[1]
    n_taps = taps.shape[0]
    scale = 1.0 / math.sqrt(rows * n_sp)
    blk = 128
    n_blk = rows // blk
    low = low_rows(ch)
    top = ch - low

    loads = [
        pltpu.make_async_copy(a, b, in_sems.at[i])
        for i, (a, b) in enumerate([(cot_h, cot), (weight_h, weight), (pv_h, pv), (pg_h, pg)])
    ]
    for c in loads:
        c.start()

    barrier = pltpu.get_barrier_semaphore()
    for i in range(1, n_sp):
        pl.semaphore_signal(barrier, inc=1, device_id=(lax.rem(s + i, n_sp), t), device_id_type=MESH)
    for i in range(1, n_tp):
        pl.semaphore_signal(barrier, inc=1, device_id=(s, lax.rem(t + i, n_tp)), device_id_type=MESH)

    row8b = lax.broadcasted_iota(jnp.int32, (8, blk), 0)

    @pl.loop(0, n_blk)
    def _(i):
        at = pl.ds(pl.multiple_of(i * blk, blk), blk)
        c = conv[:, at].astype(f32)
        stat[:, at] = jnp.where(
            row8b == 0, jnp.sum(c, axis=0, keepdims=True), jnp.sum(c * c, axis=0, keepdims=True)
        )

    pl.semaphore_wait(barrier, n_sp - 1 + n_tp - 1)

    def tp_copies(src, dst, ss, rs):
        return [
            pltpu.make_async_remote_copy(
                src_ref=src, dst_ref=dst.at[i - 1], send_sem=ss.at[i - 1], recv_sem=rs.at[i - 1],
                device_id=(s, lax.rem(t + i, n_tp)), device_id_type=MESH,
            )
            for i in range(1, n_tp)
        ]

    stat_copies = tp_copies(stat, stat_in, stat_ss, stat_rs)
    for c in stat_copies:
        c.start()

    gain_c[...] = jnp.broadcast_to(gain[...].astype(f32).reshape(1, ch), (128, ch)).T
    loads[0].wait()
    loads[1].wait()
    wide_blk = 256 if rows % 256 == 0 else 128

    @pl.loop(0, rows // wide_blk)
    def _(i):
        at = pl.ds(pl.multiple_of(i * wide_blk, wide_blk), wide_blk)
        d_act[:, at] = jnp.dot(weight[...], cot[:, at], preferred_element_type=f32)

    for c in stat_copies:
        c.wait()
    total = stat[...]
    for i in range(n_tp - 1):
        total = total + stat_in[i]
    mean = total[0:1] / width
    inv = lax.rsqrt(total[1:2] / width - mean * mean + norm_eps)
    row8 = lax.broadcasted_iota(jnp.int32, (8, rows), 0)
    cols[...] = jnp.where(row8 == 0, mean, inv)

    @pl.loop(0, n_blk)
    def _(i):
        at = pl.ds(pl.multiple_of(i * blk, blk), blk)
        c = conv[:, at].astype(f32)
        normed = (c - cols[0:1, at]) * cols[1:2, at] * gain_c[...]
        act_t[:, at] = (normed * jax.nn.sigmoid(normed)).astype(jnp.bfloat16)

    orders = line_order(n_z)
    dest = [lookup([orders[i][k] for i in range(n_z)], z) for k in range(n_z)]

    cut = top // 2 // 8 * 8
    halves = [(0, cut), (cut, top - cut)]

    def y_copy(k, h):
        at = pl.ds(*halves[h])
        sem = dest[k] * 2 + h
        return pltpu.make_async_remote_copy(
            src_ref=term.at[dest[k] * fold + other_y, at, :], dst_ref=got_y.at[dest[k], at, :],
            send_sem=y_ss.at[sem], recv_sem=y_rs.at[sem],
            device_id=(z * fold + other_y, t), device_id_type=MESH,
        )

    y_copies = [[y_copy(k, h) for h in range(2)] for k in range(n_z)]

    def make_term(j):
        term[j] = lax.dot_general(
            act_t[...], cot[j * part:(j + 1) * part, :], (((1,), (1,)), ((), ())),
            preferred_element_type=f32,
        )

    lead = dest[0] * fold + other_y
    leads = sorted({orders[i][0] * fold + o for i in range(n_z) for o in range(fold)})
    for j in leads:
        @pl.when(lead == j)
        def _():
            make_term(j)

    for h in range(2):
        y_copies[0][h].start()
    for j in range(n_sp):
        if j in leads:
            @pl.when(lead != j)
            def _():
                make_term(j)
        else:
            make_term(j)


    def line_copy(d, h, up):
        buf, ss, rs = (got_r, r_ss, r_rs) if up else (got_l, l_ss, l_rs)
        to = z + 1 if up else z - 1
        to = jnp.clip(to, 0, n_z - 1)
        return pltpu.make_async_remote_copy(
            src_ref=term.at[d * fold + y, pl.ds(*halves[h]), :], dst_ref=buf.at[d, pl.ds(*halves[h]), :],
            send_sem=ss.at[d * 2 + h], recv_sem=rs.at[d * 2 + h],
            device_id=(to * fold + y, t), device_id_type=MESH,
        )

    def add_into(d, h, buf):
        own = d * fold + y
        first, count = halves[h]
        step = max(c for c in range(8, 81, 8) if count % c == 0)

        @pl.loop(0, count // step)
        def _(i):
            at = pl.ds(pl.multiple_of(first + i * step, 8), step)
            term[own, at, :] = term[own, at, :] + buf[d, at, :]

    def hop(k, h):
        d = dest[k]
        y_copies[k][h].wait_recv()
        add_into(d, h, got_y)

        @pl.when(d > z)
        def _():
            @pl.when(z > 0)
            def _():
                line_copy(d, h, True).wait_recv()
                add_into(d, h, got_r)

            line_copy(d, h, True).start()

        @pl.when(d < z)
        def _():
            @pl.when(z < n_z - 1)
            def _():
                line_copy(d, h, False).wait_recv()
                add_into(d, h, got_l)

            line_copy(d, h, False).start()

    def low_copy(d, up):
        buf, ss, rs = (low_r, lr_ss, lr_rs) if up else (low_l, ll_ss, ll_rs)
        to = jnp.clip(z + 1 if up else z - 1, 0, n_z - 1)
        return pltpu.make_async_remote_copy(
            src_ref=term.at[pl.ds(d * fold, fold), pl.ds(top, low), :], dst_ref=buf.at[d],
            send_sem=ss.at[d], recv_sem=rs.at[d], device_id=(to * fold + y, t), device_id_type=MESH,
        )

    def low_take(d, up):
        low_copy(d, up).wait_recv()
        buf = low_r if up else low_l
        at = pl.ds(d * fold, fold)
        term[at, pl.ds(top, low), :] = term[at, pl.ds(top, low), :] + buf[d]

    def low_hop(k):
        d = dest[k]

        @pl.when(d > z)
        def _():
            @pl.when(z > 0)
            def _():
                low_take(d, True)

            low_copy(d, True).start()

        @pl.when(d < z)
        def _():
            @pl.when(z < n_z - 1)
            def _():
                low_take(d, False)

            low_copy(d, False).start()

    low_swap = pltpu.make_async_remote_copy(
        src_ref=term.at[z * fold + other_y, pl.ds(top, low), :], dst_ref=low_y,
        send_sem=ly_ss, recv_sem=ly_rs, device_id=(z * fold + other_y, t), device_id_type=MESH,
    )

    def low_end():
        @pl.when(z > 0)
        def _():
            low_take(z, True)

        @pl.when(z < n_z - 1)
        def _():
            low_take(z, False)

        low_swap.start()

    for h in range(2):
        y_copies[1][h].start()

    @pl.when(jnp.logical_or(z == 0, z == n_z - 1))
    def _():
        for k in range(n_z - 1):
            low_hop(k)

    @pl.loop(0, n_blk)
    def _(i):
        at = pl.ds(pl.multiple_of(i * blk, blk), blk)
        c = conv[:, at].astype(f32)
        centered = (c - cols[0:1, at]) * cols[1:2, at]
        normed = centered * gain_c[...]
        gate = jax.nn.sigmoid(normed)
        d_hat = d_act[:, at] * gate * (1.0 + normed * (1.0 - gate)) * gain_c[...]
        d_act[:, at] = d_hat
        mom[:, at] = jnp.where(
            row8b == 0, jnp.sum(d_hat, axis=0, keepdims=True),
            jnp.sum(d_hat * centered, axis=0, keepdims=True),
        )

    mid = jnp.logical_and(z > 0, z < n_z - 1)
    mom_copies = tp_copies(mom, mom_in, mom_ss, mom_rs)
    for c in mom_copies:
        c.start()
    for k in range(n_taps):
        taps_b[k] = jnp.broadcast_to(taps[k:k + 1, :].astype(f32), (8, ch))
    grad_acc[...] = jnp.zeros_like(grad_acc)
    loads[2].wait()
    loads[3].wait()

    @pl.loop(0, n_blk)
    def _(i):
        at = pl.ds(pl.multiple_of(i * blk, blk), blk)
        gated_s[at, :] = (pv[:, at].astype(f32) * jax.nn.sigmoid(pg[:, at].astype(f32))).T

    for c in mom_copies:
        c.wait()
    total = mom[...]
    for i in range(n_tp - 1):
        total = total + mom_in[i]
    cols2[...] = total / width

    @pl.loop(0, n_blk)
    def _(i):
        at = pl.ds(pl.multiple_of(i * blk, blk), blk)
        c = conv[:, at].astype(f32)
        inv_std = cols[1:2, at]
        centered = (c - cols[0:1, at]) * inv_std
        ext[at, :] = (inv_std * (d_act[:, at] - cols2[0:1, at] - centered * cols2[1:2, at])).T

    reach = 32
    back = jnp.maximum(s - 1, 0)
    halo = pltpu.make_async_remote_copy(
        src_ref=ext.at[pl.ds(0, reach), :], dst_ref=ext.at[pl.ds(rows, reach), :],
        send_sem=halo_ss, recv_sem=halo_rs, device_id=(back, t), device_id_type=MESH,
    )

    @pl.when(s > 0)
    def _():
        halo.start()

    for k in range(2, n_z):
        for h in range(2):
            y_copies[k][h].start()

    def shift_block(i):
        start = pl.multiple_of(i * reach, reach)
        win = ext[pl.ds(start, reach + 8), :]
        for o in range(8):
            shifted[o, pl.ds(start, reach), :] = win[o:o + reach]

    lanes = [(lo, min(128, ch - lo)) for lo in range(0, ch, 128)]

    def conv_blocks(first, last):
        for lo, wide in lanes:
            ln = slice(lo, lo + wide)

            def body(i, accs):
                start = pl.multiple_of(i * reach, reach)
                at = pl.ds(start, reach)
                gated = gated_s[at, ln]
                d_glu = jnp.zeros((reach, wide), f32)
                out = []
                for o in range(n_taps):
                    x = shifted[o % 8, pl.ds(pl.multiple_of(start + 8 * (o // 8), 8), reach), ln]
                    tap = taps_b[n_taps - 1 - o, :, ln]
                    d_glu = d_glu + jnp.concatenate([tap] * (reach // 8), axis=0) * x
                    prod = gated * x
                    acc = accs[o]
                    for q in range(reach // 8):
                        acc = acc + prod[8 * q:8 * q + 8]
                    out.append(acc)
                d_glu_s[at, ln] = d_glu
                return tuple(out)

            accs = tuple(grad_acc[n_taps - 1 - o, :, ln] for o in range(n_taps))
            accs = lax.fori_loop(first, last, body, accs)
            for o in range(n_taps):
                grad_acc[n_taps - 1 - o, :, ln] = accs[o]

    n_row = rows // reach

    @pl.when(mid)
    def _():
        for k in range(n_z - 1):
            low_hop(k)


    @pl.loop(0, n_row - 1)
    def _(i):
        shift_block(i)

    marks = [(n_row - 2) * i // 4 for i in range(5)]
    hop(0, 0)
    conv_blocks(marks[0], marks[1])
    hop(0, 1)
    low_end()
    conv_blocks(marks[1], marks[2])
    hop(1, 0)
    conv_blocks(marks[2], marks[3])
    hop(1, 1)
    conv_blocks(marks[3], marks[4])

    @pl.when(s < n_sp - 1)
    def _():
        halo.wait_recv()

    @pl.when(s == n_sp - 1)
    def _():
        ext[pl.ds(rows, reach), :] = jnp.zeros((reach, ch), f32)

    shift_block(n_row - 1)
    win = ext[pl.ds(rows, reach), :]
    for o in range(8):
        shifted[o, pl.ds(rows, reach - 8), :] = win[o:o + reach - 8]
    conv_blocks(n_row - 2, n_row)

    for k in range(n_taps):
        g_own[k:k + 1, :] = jnp.sum(grad_acc[k], axis=0, keepdims=True)
    for k in range(n_taps, g_own.shape[0]):
        g_own[k:k + 1, :] = jnp.zeros((1, ch), f32)
    gz_copies = [
        pltpu.make_async_remote_copy(
            src_ref=g_own, dst_ref=g_in.at[i - 1], send_sem=gz_ss.at[i - 1], recv_sem=gz_rs.at[i - 1],
            device_id=(lax.rem(z + i, n_z) * fold + y, t), device_id_type=MESH,
        )
        for i in range(1, n_z)
    ]
    for c in gz_copies:
        c.start()
    for k in range(2, n_z - 1):
        for h in range(2):
            hop(k, h)

    @pl.loop(0, n_blk)
    def _(i):
        at = pl.ds(pl.multiple_of(i * blk, blk), blk)
        gate = jax.nn.sigmoid(pg[:, at].astype(f32))
        d_glu = d_glu_s[at, :].T
        out_v[:, at] = (d_glu * gate).astype(jnp.bfloat16)
        out_g[:, at] = (d_glu * (pv[:, at].astype(f32) * gate) * (1.0 - gate)).astype(jnp.bfloat16)

    for c in gz_copies:
        c.wait()
    total = g_own[...]
    for i in range(n_z - 1):
        total = total + g_in[i]
    g_mid[...] = total
    gy = pltpu.make_async_remote_copy(
        src_ref=g_mid, dst_ref=g_yin, send_sem=gy_ss, recv_sem=gy_rs,
        device_id=(z * fold + other_y, t), device_id_type=MESH,
    )
    gy.start()
    for h in range(2):
        y_copies[n_z - 1][h].wait_recv()
        add_into(z, h, got_y)

        @pl.when(z > 0)
        def _():
            line_copy(z, h, True).wait_recv()
            add_into(z, h, got_r)

        @pl.when(z < n_z - 1)
        def _():
            line_copy(z, h, False).wait_recv()
            add_into(z, h, got_l)

    low_swap.wait()
    own = z * fold + y
    out_w[:top, :] = term[own, :top, :] * scale
    out_w[top:, :] = (term[own, top:, :] + low_y[...]) * scale
    gy.wait()
    out_t[...] = ((g_mid[...] + g_yin[...]) * scale)[:n_taps]
    for k in range(n_z):
        for h in range(2):
            y_copies[k][h].wait_send()

    @pl.when(s > 0)
    def _():
        halo.wait_send()

    for k in range(n_z - 1):
        d = dest[k]

        @pl.when(d > z)
        def _():
            for h in range(2):
                line_copy(d, h, True).wait_send()
            low_copy(d, True).wait_send()

        @pl.when(d < z)
        def _():
            for h in range(2):
                line_copy(d, h, False).wait_send()
            low_copy(d, False).wait_send()


def fused(n_sp, n_tp, proj_value, proj_gate, conv_saved, conv_taps, norm_gain, out_weight, cotangent):
    fold = 2
    n_z = n_sp // fold
    rows, width = cotangent.shape
    ch = conv_saved.shape[1]
    n_taps = conv_taps.shape[0]
    part = width // n_sp
    low = low_rows(ch)
    top = ch - low
    dma = pltpu.SemaphoreType.DMA
    V = pltpu.VMEM
    bf = jnp.bfloat16
    vm = pl.BlockSpec(memory_space=pltpu.VMEM)
    hb = pl.BlockSpec(memory_space=pl.ANY)
    grad_value, grad_gate, grad_weight, grad_taps = pl.pallas_call(
        functools.partial(kernel, n_sp, n_tp, fold),
        out_shape=(
            jax.ShapeDtypeStruct((ch, rows), bf),
            jax.ShapeDtypeStruct((ch, rows), bf),
            jax.ShapeDtypeStruct((ch, part), f32),
            jax.ShapeDtypeStruct((n_taps, ch), f32),
        ),
        in_specs=[hb, hb, vm, vm, vm, hb, hb],
        out_specs=[vm] * 4,
        scratch_shapes=[
            V((ch, rows), bf), V((ch, rows), bf), V((ch, width), bf), V((width, rows), bf), dma((4,)),
            V((ch, 128), f32), V((rows, ch), f32), V((rows, ch), f32),
            V((ch, rows), bf), V((ch, rows), f32), V((rows + 32, ch), f32), V((8, rows + 32, ch), f32),
            V((8, rows), f32), V((8, rows), f32),
            V((n_sp, ch, part), f32), V((n_z, top, part), f32), V((n_z, top, part), f32),
            V((n_z, top, part), f32),
            V((n_z, fold, low, part), f32), V((n_z, fold, low, part), f32), V((low, part), f32),
            V((8, rows), f32), V((n_tp - 1, 8, rows), f32), V((8, rows), f32), V((n_tp - 1, 8, rows), f32),
            V((n_taps, 8, ch), f32), V((32, ch), f32), V((32, ch), f32), V((n_z - 1, 32, ch), f32),
            V((32, ch), f32), V((n_taps, 8, ch), f32),
            dma((n_tp - 1,)), dma((n_tp - 1,)), dma((n_tp - 1,)), dma((n_tp - 1,)),
            *[dma((2 * n_z,))] * 6,
            dma((n_z,)), dma((n_z,)), dma((n_z,)), dma((n_z,)), dma, dma,
            dma, dma, dma((n_z - 1,)), dma((n_z - 1,)), dma, dma,
        ],
        compiler_params=pltpu.CompilerParams(
            collective_id=0, has_side_effects=True, vmem_limit_bytes=60 * 1024 * 1024
        ),
    )(
        proj_value.T, proj_gate.T, conv_saved.T, conv_taps, norm_gain, out_weight,
        cotangent.T,
    )
    results = (grad_value, grad_gate, grad_weight, grad_taps)
    grad_value, grad_gate, grad_weight, grad_taps = pl.pallas_call(
        finish,
        out_shape=tuple(jax.ShapeDtypeStruct(r.shape, r.dtype) for r in results),
        in_specs=[hb] * 4,
        out_specs=[hb] * 4,
        scratch_shapes=[V(r.shape, r.dtype) for r in results] + [dma((8,))],
        compiler_params=pltpu.CompilerParams(vmem_limit_bytes=60 * 1024 * 1024),
    )(*results)
    return grad_value.T, grad_gate.T, grad_weight, grad_taps


def passed_along(block, axis, distance):
    devices = range(lax.axis_size(axis))
    route = [(i - distance, i) for i in devices if i - distance in devices]
    return lax.ppermute(block, axis, route)


def local(proj_value, proj_gate, conv_saved, conv_taps, norm_gain, out_weight, cotangent):
    model_width = cotangent.shape[1]
    tok_rows = cotangent.shape[0]
    tap_count = conv_taps.shape[0]
    overhang = tap_count - 1
    grad_scale = 1.0 / math.sqrt(tok_rows * lax.axis_size("sp"))
    conv_f = conv_saved.astype(jnp.float32)
    totals = lax.psum((jnp.sum(conv_f, axis=1), jnp.sum(conv_f * conv_f, axis=1)), "tp")
    row_mean = totals[0] / model_width
    row_var = totals[1] / model_width - row_mean * row_mean
    inv_std = lax.rsqrt(row_var + norm_eps)
    centered = (conv_f - row_mean[:, None]) * inv_std[:, None]
    gain_f = norm_gain.astype(jnp.float32)
    normed = centered * gain_f
    gate_norm = jax.nn.sigmoid(normed)
    activated = (normed * gate_norm).astype(jnp.bfloat16)
    contract_rows = (((0,), (0,)), ((), ()))
    whole_term = lax.dot_general(
        cotangent, activated, contract_rows, preferred_element_type=jnp.float32
    )
    shard_grad = lax.psum_scatter(whole_term, "sp", scatter_dimension=0, tiled=True)
    grad_out_weight = shard_grad.T * grad_scale
    d_act = lax.dot_general(
        cotangent, out_weight, (((1,), (1,)), ((), ())), preferred_element_type=jnp.float32
    )
    d_hat = d_act * gate_norm * (1.0 + normed * (1.0 - gate_norm)) * gain_f
    moments = lax.psum((jnp.sum(d_hat, axis=1), jnp.sum(d_hat * centered, axis=1)), "tp")
    first = moments[0] / model_width
    second = moments[1] / model_width
    d_conv = inv_std[:, None] * (d_hat - first[:, None] - centered * second[:, None])
    ahead = passed_along(d_conv[:overhang], "sp", -1)
    extended = jnp.concatenate([d_conv, ahead], axis=0)
    gate_proj = jax.nn.sigmoid(proj_gate.astype(jnp.float32))
    gated = proj_value.astype(jnp.float32) * gate_proj
    taps_f = conv_taps.astype(jnp.float32)
    d_glu = jnp.zeros_like(d_conv)
    tap_rows = []
    for offset in range(tap_count):
        shifted = extended[overhang - offset : overhang - offset + tok_rows]
        d_glu = d_glu + taps_f[offset] * shifted
        tap_rows.append(jnp.sum(gated * shifted, axis=0))
    grad_taps = lax.psum(jnp.stack(tap_rows), "sp") * grad_scale
    grad_value = (d_glu * gate_proj).astype(jnp.bfloat16)
    grad_gate = (d_glu * gated * (1.0 - gate_proj)).astype(jnp.bfloat16)
    return (grad_value, grad_gate, grad_out_weight, grad_taps)


def solution(mesh):
    in_specs = (
        P("sp", "tp"),
        P("sp", "tp"),
        P("sp", "tp"),
        P(None, "tp"),
        P("tp"),
        P("tp", None),
        P("sp", None),
    )
    out_specs = (P("sp", "tp"), P("sp", "tp"), P("tp", "sp"), P(None, "tp"))
    n_sp, n_tp = mesh.shape["sp"], mesh.shape["tp"]

    def step(*args):
        rows, width = args[6].shape
        ch, n_taps = args[2].shape[1], args[3].shape[0]
        small = n_sp % 2 == 0 and 4 <= n_sp <= 8 and width % n_sp == 0 and n_tp > 1
        if small and rows % 128 == 0 and rows >= 128 and ch % 8 == 0 and 24 < n_taps <= 31:
            return fused(n_sp, n_tp, *args)
        return local(*args)

    return jax.shard_map(step, mesh=mesh, in_specs=in_specs, out_specs=out_specs, check_vma=False)
```

profile of v0, /device:TPU:0, one launch (start us, length us, event | category | flops | bytes accessed | tf_op | source)
XLA Modules:
  0.0 60.3 jit_solution(13156383820931967950)
XLA Ops:
  0.6 57.4 %shard_map.102 = (bf16[504,512]{1,0:T(8,128)(2,1)}, bf16[504,512]{1,0:T(8,128)(2,1)}, f32[504,252]{1,0:T(8,128)}, f32[31,504]{1,0:T(8,128)}) custom-call(bf16[504,512]{1,0:T(8,128)(2,1)} %bitcast.7, bf16[504,512]{1,0:T(8,128)(2,1)} %bitcast.8, bf16[504,512]{1,0:T(8,128)(2,1)} %bitcast.9, bf16[31,504]{1,0:T(8,128)(2,1)} %taps.1, bf16[504]{0:T(512)(128)(2,1)} %gain.1, ...), custom_call_target="tpu_custom_call" | custom-call | tf_op jit(solution)/shard_map/pallas_call | solution.py:504
  58.0 2.2 %shard_map.103 = (bf16[504,512]{1,0:T(8,128)(2,1)}, bf16[504,512]{1,0:T(8,128)(2,1)}, f32[504,252]{1,0:T(8,128)}, f32[31,504]{1,0:T(8,128)}) custom-call(bf16[504,512]{1,0:T(8,128)(2,1)} %get-tuple-element.12.v_in, bf16[504,512]{1,0:T(8,128)(2,1)} %get-tuple-element.13.g_in, f32[504,252]{1,0:T(8,128)} %get-tuple-element.14.w_in, ...), custom_call_target="tpu_custom_call" | custom-call | tf_op jit(solution)/shard_map/pallas_call | solution.py:538
where the time goes:
time: 61 us; the launch traced here: 60.3 us
  Pallas kernels  59.6 us (98%)
  between operations  0.64 us (1%)
    pallas_call x1, Pallas kernels, fused(): pl.pallas_call(functools.partial(kernel, n_sp, n_tp, fold), out_shape=(ja...  57.4 us
    pallas_call x1, Pallas kernels, fused(): pl.pallas_call(finish, out_shape=tuple((jax.ShapeDtypeStruct(r.shape, r.d...  2.25 us

commit v1 on v0

--- a/solution.py
+++ b/solution.py
@@ -11,6 +11,7 @@
 norm_eps = 1e-05
 MESH = pl.DeviceIdType.MESH
 f32 = jnp.float32
+pieces = 4
 
 
 def line_order(length):
@@ -21,8 +22,9 @@
     return rows
 
 
-def low_rows(ch):
-    return max(ch // 7 // 8 * 8, 8)
+def split_rows(ch):
+    chunk = max((ch * 33 + 640) // 1280, 1) * 8
+    return chunk * pieces, ch - chunk * pieces
 
 
 def lookup(table, place):
@@ -32,27 +34,23 @@
     return value
 
 
-def finish(v_in, g_in, w_in, t_in, v_out, g_out, w_out, t_out, v_b, g_b, w_b, t_b, ss):
-    trips = [(v_in, v_b, v_out), (g_in, g_b, g_out), (w_in, w_b, w_out), (t_in, t_b, t_out)]
-    inward = [pltpu.make_async_copy(a, b, ss.at[i]) for i, (a, b, _) in enumerate(trips)]
-    outward = [pltpu.make_async_copy(b, c, ss.at[4 + i]) for i, (_, b, c) in enumerate(trips)]
-    for c in inward:
+def finish(v_in, g_in, w_in, t_in, v_out, g_out, w_out, t_out, ss):
+    pairs = [(v_in, v_out), (g_in, g_out), (w_in, w_out), (t_in, t_out)]
+    copies = [pltpu.make_async_copy(a, b, ss.at[i]) for i, (a, b) in enumerate(pairs)]
+    for c in copies:
         c.start()
-    for a, b in zip(inward, outward):
-        a.wait()
-        b.start()
-    for b in outward:
-        b.wait()
+    for c in copies:
+        c.wait()
 
 
 def kernel(
     n_sp, n_tp, fold, pv_h, pg_h, conv, taps, gain, weight_h, cot_h,
     out_v, out_g, out_w, out_t,
     pv, pg, weight, cot, in_sems, gain_c, gated_s, d_glu_s, act_t, d_act, ext, shifted, cols, cols2, term, got_y, got_r, got_l, low_r, low_l, low_y,
-    stat, stat_in, mom, mom_in, grad_acc, g_own, g_mid, g_in, g_yin, taps_b,
+    stat, stat_in, mom, mom_in, grad_acc, g_own, g_mid, g_up, g_dn, g_up_out, g_dn_out, g_yin, taps_b,
     stat_ss, stat_rs, mom_ss, mom_rs, y_ss, y_rs, r_ss, r_rs, l_ss, l_rs,
     lr_ss, lr_rs, ll_ss, ll_rs, ly_ss, ly_rs,
-    halo_ss, halo_rs, gz_ss, gz_rs, gy_ss, gy_rs,
+    halo_ss, halo_rs, gu_ss, gu_rs, gd_ss, gd_rs, gy_ss, gy_rs,
 ):
     s = lax.axis_index("sp")
     t = lax.axis_index("tp")
@@ -67,8 +65,9 @@
     scale = 1.0 / math.sqrt(rows * n_sp)
     blk = 128
     n_blk = rows // blk
-    low = low_rows(ch)
-    top = ch - low
+    top, low = split_rows(ch)
+    end = jnp.logical_or(z == 0, z == n_z - 1)
+    mid = jnp.logical_and(z > 0, z < n_z - 1)
 
     loads = [
         pltpu.make_async_copy(a, b, in_sems.at[i])
@@ -78,22 +77,47 @@
         c.start()
 
     barrier = pltpu.get_barrier_semaphore()
-    for i in range(1, n_sp):
-        pl.semaphore_signal(barrier, inc=1, device_id=(lax.rem(s + i, n_sp), t), device_id_type=MESH)
+
+    def greet(s_to, t_to):
+        pl.semaphore_signal(barrier, inc=1, device_id=(s_to, t_to), device_id_type=MESH)
+
     for i in range(1, n_tp):
-        pl.semaphore_signal(barrier, inc=1, device_id=(s, lax.rem(t + i, n_tp)), device_id_type=MESH)
-
-    row8b = lax.broadcasted_iota(jnp.int32, (8, blk), 0)
+        greet(s, lax.rem(t + i, n_tp))
+    greet(z * fold + other_y, t)
+
+    @pl.when(z > 0)
+    def _():
+        greet(s - fold, t)
+
+        @pl.when(y == 0)
+        def _():
+            greet(s - 1, t)
+
+    @pl.when(z < n_z - 1)
+    def _():
+        greet(s + fold, t)
+
+        @pl.when(y == fold - 1)
+        def _():
+            greet(s + 1, t)
+
+    def put_sums(ref, i, first, second):
+        ref[pl.ds(i, 1), :] = jnp.sum(first, axis=0, keepdims=True)
+        ref[pl.ds(n_blk + i, 1), :] = jnp.sum(second, axis=0, keepdims=True)
+
+    if stat.shape[0] > 2 * n_blk:
+        stat[...] = jnp.zeros_like(stat)
+        mom[...] = jnp.zeros_like(mom)
 
     @pl.loop(0, n_blk)
     def _(i):
         at = pl.ds(pl.multiple_of(i * blk, blk), blk)
         c = conv[:, at].astype(f32)
-        stat[:, at] = jnp.where(
-            row8b == 0, jnp.sum(c, axis=0, keepdims=True), jnp.sum(c * c, axis=0, keepdims=True)
-        )
-
-    pl.semaphore_wait(barrier, n_sp - 1 + n_tp - 1)
+        put_sums(stat, i, c, c * c)
+
+    below = jnp.where(z > 0, jnp.where(y == 0, 2, 1), 0)
+    above = jnp.where(z < n_z - 1, jnp.where(y == fold - 1, 2, 1), 0)
+    pl.semaphore_wait(barrier, n_tp + below + above)
 
     def tp_copies(src, dst, ss, rs):
         return [
@@ -123,10 +147,11 @@
     total = stat[...]
     for i in range(n_tp - 1):
         total = total + stat_in[i]
-    mean = total[0:1] / width
-    inv = lax.rsqrt(total[1:2] / width - mean * mean + norm_eps)
-    row8 = lax.broadcasted_iota(jnp.int32, (8, rows), 0)
-    cols[...] = jnp.where(row8 == 0, mean, inv)
+    mean = total[:n_blk] / width
+    inv = lax.rsqrt(total[n_blk:2 * n_blk] / width - mean * mean + norm_eps)
+    for i in range(n_blk):
+        cols[0:1, i * blk:(i + 1) * blk] = mean[i:i + 1]
+        cols[1:2, i * blk:(i + 1) * blk] = inv[i:i + 1]
 
     @pl.loop(0, n_blk)
     def _(i):
@@ -138,19 +163,24 @@
     orders = line_order(n_z)
     dest = [lookup([orders[i][k] for i in range(n_z)], z) for k in range(n_z)]
 
-    cut = top // 2 // 8 * 8
-    halves = [(0, cut), (cut, top - cut)]
+    chunk = top // pieces
+
+    def piece(h):
+        return pl.ds(h * chunk, chunk)
 
     def y_copy(k, h):
-        at = pl.ds(*halves[h])
-        sem = dest[k] * 2 + h
+        sem = dest[k] * pieces + h
         return pltpu.make_async_remote_copy(
-            src_ref=term.at[dest[k] * fold + other_y, at, :], dst_ref=got_y.at[dest[k], at, :],
+            src_ref=term.at[dest[k] * fold + other_y, piece(h), :], dst_ref=got_y.at[dest[k], piece(h), :],
             send_sem=y_ss.at[sem], recv_sem=y_rs.at[sem],
             device_id=(z * fold + other_y, t), device_id_type=MESH,
         )
 
-    y_copies = [[y_copy(k, h) for h in range(2)] for k in range(n_z)]
+    y_copies = [[y_copy(k, h) for h in range(pieces)] for k in range(n_z)]
+
+    def y_start(k, first=0, last=pieces):
+        for h in range(first, last):
+            y_copies[k][h].start()
 
     def make_term(j):
         term[j] = lax.dot_general(
@@ -159,42 +189,28 @@
         )
 
     lead = dest[0] * fold + other_y
+    second = dest[0] * fold + y
     leads = sorted({orders[i][0] * fold + o for i in range(n_z) for o in range(fold)})
-    for j in leads:
-        @pl.when(lead == j)
-        def _():
-            make_term(j)
-
-    for h in range(2):
-        y_copies[0][h].start()
-    for j in range(n_sp):
-        if j in leads:
-            @pl.when(lead != j)
+
+    def make_one_of(place):
+        for j in leads:
+            @pl.when(place == j)
             def _():
                 make_term(j)
-        else:
-            make_term(j)
-
 
     def line_copy(d, h, up):
         buf, ss, rs = (got_r, r_ss, r_rs) if up else (got_l, l_ss, l_rs)
         to = z + 1 if up else z - 1
         to = jnp.clip(to, 0, n_z - 1)
         return pltpu.make_async_remote_copy(
-            src_ref=term.at[d * fold + y, pl.ds(*halves[h]), :], dst_ref=buf.at[d, pl.ds(*halves[h]), :],
-            send_sem=ss.at[d * 2 + h], recv_sem=rs.at[d * 2 + h],
+            src_ref=term.at[d * fold + y, piece(h), :], dst_ref=buf.at[d, piece(h), :],
+            send_sem=ss.at[d * pieces + h], recv_sem=rs.at[d * pieces + h],
             device_id=(to * fold + y, t), device_id_type=MESH,
         )
 
     def add_into(d, h, buf):
         own = d * fold + y
-        first, count = halves[h]
-        step = max(c for c in range(8, 81, 8) if count % c == 0)
-
-        @pl.loop(0, count // step)
-        def _(i):
-            at = pl.ds(pl.multiple_of(first + i * step, 8), step)
-            term[own, at, :] = term[own, at, :] + buf[d, at, :]
+        term[own, piece(h), :] = term[own, piece(h), :] + buf[d, piece(h), :]
 
     def hop(k, h):
         d = dest[k]
@@ -268,12 +284,25 @@
 
         low_swap.start()
 
-    for h in range(2):
-        y_copies[1][h].start()
-
-    @pl.when(jnp.logical_or(z == 0, z == n_z - 1))
-    def _():
-        for k in range(n_z - 1):
+    make_one_of(lead)
+    y_start(0)
+    make_one_of(second)
+
+    @pl.when(end)
+    def _():
+        low_hop(0)
+
+    for j in range(n_sp):
+        if j in leads:
+            @pl.when(jnp.logical_and(lead != j, second != j))
+            def _():
+                make_term(j)
+        else:
+            make_term(j)
+
+    @pl.when(end)
+    def _():
+        for k in range(1, n_z - 1):
             low_hop(k)
 
     @pl.loop(0, n_blk)
@@ -285,12 +314,8 @@
         gate = jax.nn.sigmoid(normed)
         d_hat = d_act[:, at] * gate * (1.0 + normed * (1.0 - gate)) * gain_c[...]
         d_act[:, at] = d_hat
-        mom[:, at] = jnp.where(
-            row8b == 0, jnp.sum(d_hat, axis=0, keepdims=True),
-            jnp.sum(d_hat * centered, axis=0, keepdims=True),
-        )
-
-    mid = jnp.logical_and(z > 0, z < n_z - 1)
+        put_sums(mom, i, d_hat, d_hat * centered)
+
     mom_copies = tp_copies(mom, mom_in, mom_ss, mom_rs)
     for c in mom_copies:
         c.start()
@@ -310,7 +335,10 @@
     total = mom[...]
     for i in range(n_tp - 1):
         total = total + mom_in[i]
-    cols2[...] = total / width
+    total = total / width
+    for i in range(n_blk):
+        cols2[0:1, i * blk:(i + 1) * blk] = total[i:i + 1]
+        cols2[1:2, i * blk:(i + 1) * blk] = total[n_blk + i:n_blk + i + 1]
 
     @pl.loop(0, n_blk)
     def _(i):
@@ -331,9 +359,7 @@
     def _():
         halo.start()
 
-    for k in range(2, n_z):
-        for h in range(2):
-            y_copies[k][h].start()
+    y_start(1)
 
     def shift_block(i):
         start = pl.multiple_of(i * reach, reach)
@@ -372,26 +398,23 @@
 
     n_row = rows // reach
 
-    @pl.when(mid)
-    def _():
-        for k in range(n_z - 1):
-            low_hop(k)
-
-
     @pl.loop(0, n_row - 1)
     def _(i):
         shift_block(i)
 
-    marks = [(n_row - 2) * i // 4 for i in range(5)]
-    hop(0, 0)
-    conv_blocks(marks[0], marks[1])
-    hop(0, 1)
-    low_end()
-    conv_blocks(marks[1], marks[2])
-    hop(1, 0)
-    conv_blocks(marks[2], marks[3])
-    hop(1, 1)
-    conv_blocks(marks[3], marks[4])
+    half = (n_row - 2) // 2
+    conv_blocks(0, half)
+
+    @pl.when(end)
+    def _():
+        hop(0, 0)
+        hop(0, 1)
+
+    @pl.when(mid)
+    def _():
+        low_hop(0)
+
+    conv_blocks(half, n_row - 2)
 
     @pl.when(s < n_sp - 1)
     def _():
@@ -411,18 +434,33 @@
         g_own[k:k + 1, :] = jnp.sum(grad_acc[k], axis=0, keepdims=True)
     for k in range(n_taps, g_own.shape[0]):
         g_own[k:k + 1, :] = jnp.zeros((1, ch), f32)
-    gz_copies = [
-        pltpu.make_async_remote_copy(
-            src_ref=g_own, dst_ref=g_in.at[i - 1], send_sem=gz_ss.at[i - 1], recv_sem=gz_rs.at[i - 1],
-            device_id=(lax.rem(z + i, n_z) * fold + y, t), device_id_type=MESH,
+
+    def taps_copy(src, up):
+        dst, ss, rs = (g_up, gu_ss, gu_rs) if up else (g_dn, gd_ss, gd_rs)
+        to = jnp.clip(z + 1 if up else z - 1, 0, n_z - 1)
+        return pltpu.make_async_remote_copy(
+            src_ref=src, dst_ref=dst, send_sem=ss, recv_sem=rs,
+            device_id=(to * fold + y, t), device_id_type=MESH,
         )
-        for i in range(1, n_z)
-    ]
-    for c in gz_copies:
-        c.start()
-    for k in range(2, n_z - 1):
-        for h in range(2):
-            hop(k, h)
+
+    def taps_pass(up):
+        src = g_up if up else g_dn
+        out = g_up_out if up else g_dn_out
+        taps_copy(g_own, up).wait_recv()
+        out[...] = g_own[...] + src[...]
+        taps_copy(out, up).start()
+
+    @pl.when(z == 0)
+    def _():
+        g_up[...] = jnp.zeros_like(g_up)
+        taps_copy(g_own, True).start()
+
+    @pl.when(z == n_z - 1)
+    def _():
+        g_dn[...] = jnp.zeros_like(g_dn)
+        taps_copy(g_own, False).start()
+
+    y_start(2, 0, pieces if n_z > 3 else 2)
 
     @pl.loop(0, n_blk)
     def _(i):
@@ -432,18 +470,80 @@
         out_v[:, at] = (d_glu * gate).astype(jnp.bfloat16)
         out_g[:, at] = (d_glu * (pv[:, at].astype(f32) * gate) * (1.0 - gate)).astype(jnp.bfloat16)
 
-    for c in gz_copies:
-        c.wait()
-    total = g_own[...]
-    for i in range(n_z - 1):
-        total = total + g_in[i]
-    g_mid[...] = total
+    @pl.when(end)
+    def _():
+        hop(0, 2)
+        hop(0, 3)
+        for k in range(1, n_z - 2):
+            for h in range(pieces):
+                hop(k, h)
+
+    @pl.when(mid)
+    def _():
+        for k in range(n_z - 2, 0, -1):
+            low_hop(k)
+        hop(0, 0)
+        hop(0, 1)
+
+        @pl.when(2 * z < n_z)
+        def _():
+            taps_pass(True)
+
+        @pl.when(2 * z >= n_z)
+        def _():
+            taps_pass(False)
+
+        hop(0, 2)
+        hop(0, 3)
+
+    low_end()
+    if n_z > 3:
+        y_start(n_z - 1, 0, 2)
+
+    @pl.when(end)
+    def _():
+        for h in range(pieces):
+            hop(n_z - 2, h)
+
+    @pl.when(mid)
+    def _():
+        @pl.when(2 * z < n_z)
+        def _():
+            taps_pass(False)
+
+        @pl.when(2 * z >= n_z)
+        def _():
+            taps_pass(True)
+
+        for h in range(pieces):
+            hop(1, h)
+
+    @pl.when(z == 0)
+    def _():
+        taps_copy(g_own, False).wait_recv()
+
+    @pl.when(z == n_z - 1)
+    def _():
+        taps_copy(g_own, True).wait_recv()
+
+    g_mid[...] = g_own[...] + g_up[...] + g_dn[...]
     gy = pltpu.make_async_remote_copy(
         src_ref=g_mid, dst_ref=g_yin, send_sem=gy_ss, recv_sem=gy_rs,
         device_id=(z * fold + other_y, t), device_id_type=MESH,
     )
     gy.start()
-    for h in range(2):
+    y_start(n_z - 1, 2, pieces)
+
+    @pl.when(mid)
+    def _():
+        for k in range(2, n_z - 1):
+            for h in range(pieces):
+                hop(k, h)
+
+    own = z * fold + y
+    low_swap.wait()
+    out_w[top:, :] = (term[own, top:, :] + low_y[...]) * scale
+    for h in range(pieces):
         y_copies[n_z - 1][h].wait_recv()
         add_into(z, h, got_y)
 
@@ -457,15 +557,21 @@
             line_copy(z, h, False).wait_recv()
             add_into(z, h, got_l)
 
-    low_swap.wait()
-    own = z * fold + y
-    out_w[:top, :] = term[own, :top, :] * scale
-    out_w[top:, :] = (term[own, top:, :] + low_y[...]) * scale
+        out_w[piece(h), :] = term[own, piece(h), :] * scale
+
     gy.wait()
     out_t[...] = ((g_mid[...] + g_yin[...]) * scale)[:n_taps]
     for k in range(n_z):
-        for h in range(2):
+        for h in range(pieces):
             y_copies[k][h].wait_send()
+
+    @pl.when(z < n_z - 1)
+    def _():
+        taps_copy(g_own, True).wait_send()
+
+    @pl.when(z > 0)
+    def _():
+        taps_copy(g_own, False).wait_send()
 
     @pl.when(s > 0)
     def _():
@@ -476,13 +582,13 @@
 
         @pl.when(d > z)
         def _():
-            for h in range(2):
+            for h in range(pieces):
                 line_copy(d, h, True).wait_send()
             low_copy(d, True).wait_send()
 
         @pl.when(d < z)
         def _():
-            for h in range(2):
+            for h in range(pieces):
                 line_copy(d, h, False).wait_send()
             low_copy(d, False).wait_send()
 
@@ -494,8 +600,8 @@
     ch = conv_saved.shape[1]
     n_taps = conv_taps.shape[0]
     part = width // n_sp
-    low = low_rows(ch)
-    top = ch - low
+    top, low = split_rows(ch)
+    sums = -(-2 * (rows // 128) // 8) * 8
     dma = pltpu.SemaphoreType.DMA
     V = pltpu.VMEM
     bf = jnp.bfloat16
@@ -503,12 +609,7 @@
     hb = pl.BlockSpec(memory_space=pl.ANY)
     grad_value, grad_gate, grad_weight, grad_taps = pl.pallas_call(
         functools.partial(kernel, n_sp, n_tp, fold),
-        out_shape=(
-            jax.ShapeDtypeStruct((ch, rows), bf),
-            jax.ShapeDtypeStruct((ch, rows), bf),
-            jax.ShapeDtypeStruct((ch, part), f32),
-            jax.ShapeDtypeStruct((n_taps, ch), f32),
-        ),
+        out_shape=(V((ch, rows), bf), V((ch, rows), bf), V((ch, part), f32), V((n_taps, ch), f32)),
         in_specs=[hb, hb, vm, vm, vm, hb, hb],
         out_specs=[vm] * 4,
         scratch_shapes=[
@@ -519,16 +620,16 @@
             V((n_sp, ch, part), f32), V((n_z, top, part), f32), V((n_z, top, part), f32),
             V((n_z, top, part), f32),
             V((n_z, fold, low, part), f32), V((n_z, fold, low, part), f32), V((low, part), f32),
-            V((8, rows), f32), V((n_tp - 1, 8, rows), f32), V((8, rows), f32), V((n_tp - 1, 8, rows), f32),
-            V((n_taps, 8, ch), f32), V((32, ch), f32), V((32, ch), f32), V((n_z - 1, 32, ch), f32),
-            V((32, ch), f32), V((n_taps, 8, ch), f32),
+            V((sums, 128), f32), V((n_tp - 1, sums, 128), f32),
+            V((sums, 128), f32), V((n_tp - 1, sums, 128), f32),
+            V((n_taps, 8, ch), f32), *[V((32, ch), f32)] * 7, V((n_taps, 8, ch), f32),
             dma((n_tp - 1,)), dma((n_tp - 1,)), dma((n_tp - 1,)), dma((n_tp - 1,)),
-            *[dma((2 * n_z,))] * 6,
+            *[dma((pieces * n_z,))] * 6,
             dma((n_z,)), dma((n_z,)), dma((n_z,)), dma((n_z,)), dma, dma,
-            dma, dma, dma((n_z - 1,)), dma((n_z - 1,)), dma, dma,
+            *[dma] * 8,
         ],
         compiler_params=pltpu.CompilerParams(
-            collective_id=0, has_side_effects=True, vmem_limit_bytes=60 * 1024 * 1024
+            collective_id=0, has_side_effects=True, vmem_limit_bytes=56 * 1024 * 1024
         ),
     )(
         proj_value.T, proj_gate.T, conv_saved.T, conv_taps, norm_gain, out_weight,
@@ -538,11 +639,10 @@
     grad_value, grad_gate, grad_weight, grad_taps = pl.pallas_call(
         finish,
         out_shape=tuple(jax.ShapeDtypeStruct(r.shape, r.dtype) for r in results),
-        in_specs=[hb] * 4,
+        in_specs=[vm] * 4,
         out_specs=[hb] * 4,
-        scratch_shapes=[V(r.shape, r.dtype) for r in results] + [dma((8,))],
-        compiler_params=pltpu.CompilerParams(vmem_limit_bytes=60 * 1024 * 1024),
-    )(*results)
+        scratch_shapes=[dma((4,))],
+    )(*[pltpu.with_memory_space_constraint(r, pltpu.VMEM) for r in results])
     return grad_value.T, grad_gate.T, grad_weight, grad_taps
 
 
@@ -615,8 +715,8 @@
     def step(*args):
         rows, width = args[6].shape
         ch, n_taps = args[2].shape[1], args[3].shape[0]
-        small = n_sp % 2 == 0 and 4 <= n_sp <= 8 and width % n_sp == 0 and n_tp > 1
-        if small and rows % 128 == 0 and rows >= 128 and ch % 8 == 0 and 24 < n_taps <= 31:
+        small = n_sp % 2 == 0 and 6 <= n_sp <= 8 and width % n_sp == 0 and n_tp > 1
+        if small and rows % 128 == 0 and rows >= 128 and ch % 8 == 0 and ch >= 64 and 24 < n_taps <= 31:
             return fused(n_sp, n_tp, *args)
         return local(*args)
 

time: 61 us -> 54.9 us (0.900)
  Pallas kernels: 59.6 us -> 54.1 us
    pallas_call x1, Pallas kernels: 57.4 us -> 53 us  [fused(): pl.pallas_call(functools.partial(kernel, n_sp, n_tp, fold), out_shape=(V(...]
    pallas_call x1, Pallas kernels: 2.25 us -> 1.18 us  [fused(): pl.pallas_call(finish, out_shape=tuple((jax.ShapeDtypeStruct(r.shape, r.d...]
where the time goes in v1:
time: 54.9 us; the launch traced here: 54.8 us
  Pallas kernels  54.1 us (99%)
  between operations  0.64 us (1%)
    pallas_call x1, Pallas kernels, fused(): pl.pallas_call(functools.partial(kernel, n_sp, n_tp, fold), out_shape=(V(...  53 us
    pallas_call x1, Pallas kernels, fused(): pl.pallas_call(finish, out_shape=tuple((jax.ShapeDtypeStruct(r.shape, r.d...  1.18 us

profile of v1, /device:TPU:0, one launch (start us, length us, event | category | flops | bytes accessed | tf_op | source)
XLA Modules:
  0.0 54.8 jit_solution(5604590429849550135)
XLA Ops:
  0.6 53.0 %shard_map.102 = (bf16[504,512]{1,0:T(8,128)(2,1)S(1)}, bf16[504,512]{1,0:T(8,128)(2,1)S(1)}, f32[504,252]{1,0:T(8,128)S(1)}, f32[31,504]{1,0:T(8,128)S(1)}) custom-call(bf16[504,512]{1,0:T(8,128)(2,1)} %bitcast.7, bf16[504,512]{1,0:T(8,128)(2,1)} %bitcast.8, bf16[504,512]{1,0:T(8,128)(2,1)} %bitcast.9, bf16[31,504]{1,0:T(8,128)(2,1)} %taps.1, ...), custom_call_target="tpu_custom_call" | custom-call | tf_op jit(solution)/shard_map/pallas_call | solution.py:610
  53.6 1.2 %shard_map.103 = (bf16[504,512]{1,0:T(8,128)(2,1)}, bf16[504,512]{1,0:T(8,128)(2,1)}, f32[504,252]{1,0:T(8,128)}, f32[31,504]{1,0:T(8,128)}) custom-call(bf16[504,512]{1,0:T(8,128)(2,1)S(1)} %get-tuple-element.12.v_in, bf16[504,512]{1,0:T(8,128)(2,1)S(1)} %get-tuple-element.13.g_in, f32[504,252]{1,0:T(8,128)S(1)} %get-tuple-element.14.w_in, ...), custom_call_target="tpu_custom_call" | custom-call | tf_op jit(solution)/shard_map/pallas_call | solution.py:639

commit v2 on v1

--- a/solution.py
+++ b/solution.py
@@ -23,8 +23,9 @@
 
 
 def split_rows(ch):
-    chunk = max((ch * 33 + 640) // 1280, 1) * 8
-    return chunk * pieces, ch - chunk * pieces
+    units = ch * 17 // 20 // 8
+    sizes = [8 * (units // pieces + (i < units % pieces)) for i in range(pieces)]
+    return sizes, sum(sizes), ch - sum(sizes)
 
 
 def lookup(table, place):
@@ -44,13 +45,13 @@
 
 
 def kernel(
-    n_sp, n_tp, fold, pv_h, pg_h, conv, taps, gain, weight_h, cot_h,
+    n_sp, n_tp, fold, pv_h, pg_h, conv_h, taps_h, gain_h, weight_h, cot_h,
     out_v, out_g, out_w, out_t,
-    pv, pg, weight, cot, in_sems, gain_c, gated_s, d_glu_s, act_t, d_act, ext, shifted, cols, cols2, term, got_y, got_r, got_l, low_r, low_l, low_y,
-    stat, stat_in, mom, mom_in, grad_acc, g_own, g_mid, g_up, g_dn, g_up_out, g_dn_out, g_yin, taps_b,
-    stat_ss, stat_rs, mom_ss, mom_rs, y_ss, y_rs, r_ss, r_rs, l_ss, l_rs,
-    lr_ss, lr_rs, ll_ss, ll_rs, ly_ss, ly_rs,
-    halo_ss, halo_rs, gu_ss, gu_rs, gd_ss, gd_rs, gy_ss, gy_rs,
+    conv, taps, gain, pv, pg, weight, cot, in_sems, gain_c, gated_s, d_glu_s, act_t, d_act, ext, shifted, cols, cols2, term, got_y, got_line, low_in, low_y,
+    stat, stat_in, mom, mom_in, grad_acc, g_own, g_mid, g_up, g_dn, g_up_out, g_dn_out, g_yin, taps_b, edge_out, edge_in, edge_sums, edge_sums_in,
+    stat_ss, stat_rs, mom_ss, mom_rs, y_ss, y_rs, line_ss, line_rs,
+    low_ss, low_rs, ly_ss, ly_rs, edge_ss, edge_rs,
+    gu_ss, gu_rs, gd_ss, gd_rs, gy_ss, gy_rs,
 ):
     s = lax.axis_index("sp")
     t = lax.axis_index("tp")
@@ -65,16 +66,17 @@
     scale = 1.0 / math.sqrt(rows * n_sp)
     blk = 128
     n_blk = rows // blk
-    top, low = split_rows(ch)
+    sizes, top, low = split_rows(ch)
     end = jnp.logical_or(z == 0, z == n_z - 1)
     mid = jnp.logical_and(z > 0, z < n_z - 1)
 
     loads = [
         pltpu.make_async_copy(a, b, in_sems.at[i])
-        for i, (a, b) in enumerate([(cot_h, cot), (weight_h, weight), (pv_h, pv), (pg_h, pg)])
+        for i, (a, b) in enumerate([
+            (cot_h, cot), (weight_h, weight), (pv_h, pv), (pg_h, pg), (conv_h, conv), (gain_h, gain), (taps_h, taps)
+        ])
     ]
-    for c in loads:
-        c.start()
+    loads[4].start()
 
     barrier = pltpu.get_barrier_semaphore()
 
@@ -101,6 +103,9 @@
         def _():
             greet(s + 1, t)
 
+    for i in (0, 1, 5, 2, 3, 6):
+        loads[i].start()
+
     def put_sums(ref, i, first, second):
         ref[pl.ds(i, 1), :] = jnp.sum(first, axis=0, keepdims=True)
         ref[pl.ds(n_blk + i, 1), :] = jnp.sum(second, axis=0, keepdims=True)
@@ -108,6 +113,8 @@
     if stat.shape[0] > 2 * n_blk:
         stat[...] = jnp.zeros_like(stat)
         mom[...] = jnp.zeros_like(mom)
+
+    loads[4].wait()
 
     @pl.loop(0, n_blk)
     def _(i):
@@ -122,28 +129,54 @@
     def tp_copies(src, dst, ss, rs):
         return [
             pltpu.make_async_remote_copy(
-                src_ref=src, dst_ref=dst.at[i - 1], send_sem=ss.at[i - 1], recv_sem=rs.at[i - 1],
+                src_ref=src, dst_ref=dst.at[i - 1], send_sem=ss, recv_sem=rs,
                 device_id=(s, lax.rem(t + i, n_tp)), device_id_type=MESH,
             )
             for i in range(1, n_tp)
         ]
 
-    stat_copies = tp_copies(stat, stat_in, stat_ss, stat_rs)
-    for c in stat_copies:
+    def tp_wait(dst, ss, rs):
+        pltpu.make_async_remote_copy(
+            src_ref=dst, dst_ref=dst, send_sem=ss, recv_sem=rs,
+            device_id=(s, lax.rem(t + 1, n_tp)), device_id_type=MESH,
+        ).wait()
+
+    for c in tp_copies(stat, stat_in, stat_ss, stat_rs):
         c.start()
 
+    reach = 32
+    back = jnp.maximum(s - 1, 0)
+
+    def edge_copy(i):
+        src, dst = (edge_sums, edge_sums_in) if i == 2 else (edge_out.at[i], edge_in.at[i])
+        return pltpu.make_async_remote_copy(
+            src_ref=src, dst_ref=dst, send_sem=edge_ss.at[i], recv_sem=edge_rs.at[i],
+            device_id=(back, t), device_id_type=MESH,
+        )
+
+    def edge_send(i):
+        @pl.when(s > 0)
+        def _():
+            edge_copy(i).start()
+
+    edge_out[0] = conv[:, :blk].astype(f32).T[:reach]
+    edge_send(0)
+    loads[5].wait()
     gain_c[...] = jnp.broadcast_to(gain[...].astype(f32).reshape(1, ch), (128, ch)).T
     loads[0].wait()
     loads[1].wait()
     wide_blk = 256 if rows % 256 == 0 else 128
 
-    @pl.loop(0, rows // wide_blk)
+    d_act[:, :wide_blk] = jnp.dot(weight[...], cot[:, :wide_blk], preferred_element_type=f32)
+    edge_out[1] = d_act[:, :blk].T[:reach]
+    edge_send(1)
+
+    @pl.loop(1, rows // wide_blk)
     def _(i):
         at = pl.ds(pl.multiple_of(i * wide_blk, wide_blk), wide_blk)
         d_act[:, at] = jnp.dot(weight[...], cot[:, at], preferred_element_type=f32)
 
-    for c in stat_copies:
-        c.wait()
+    tp_wait(stat_in, stat_ss, stat_rs)
     total = stat[...]
     for i in range(n_tp - 1):
         total = total + stat_in[i]
@@ -153,26 +186,19 @@
         cols[0:1, i * blk:(i + 1) * blk] = mean[i:i + 1]
         cols[1:2, i * blk:(i + 1) * blk] = inv[i:i + 1]
 
-    @pl.loop(0, n_blk)
-    def _(i):
-        at = pl.ds(pl.multiple_of(i * blk, blk), blk)
-        c = conv[:, at].astype(f32)
-        normed = (c - cols[0:1, at]) * cols[1:2, at] * gain_c[...]
-        act_t[:, at] = (normed * jax.nn.sigmoid(normed)).astype(jnp.bfloat16)
-
     orders = line_order(n_z)
     dest = [lookup([orders[i][k] for i in range(n_z)], z) for k in range(n_z)]
 
-    chunk = top // pieces
+    firsts = [sum(sizes[:h]) for h in range(pieces)]
 
     def piece(h):
-        return pl.ds(h * chunk, chunk)
+        return pl.ds(firsts[h], sizes[h])
 
     def y_copy(k, h):
         sem = dest[k] * pieces + h
         return pltpu.make_async_remote_copy(
             src_ref=term.at[dest[k] * fold + other_y, piece(h), :], dst_ref=got_y.at[dest[k], piece(h), :],
-            send_sem=y_ss.at[sem], recv_sem=y_rs.at[sem],
+            send_sem=y_ss, recv_sem=y_rs.at[sem],
             device_id=(z * fold + other_y, t), device_id_type=MESH,
         )
 
@@ -182,9 +208,9 @@
         for h in range(first, last):
             y_copies[k][h].start()
 
-    def make_term(j):
-        term[j] = lax.dot_general(
-            act_t[...], cot[j * part:(j + 1) * part, :], (((1,), (1,)), ((), ())),
+    def make_term(j, at=slice(None)):
+        term[j, at, :] = lax.dot_general(
+            act_t[at, :], cot[j * part:(j + 1) * part, :], (((1,), (1,)), ((), ())),
             preferred_element_type=f32,
         )
 
@@ -192,37 +218,40 @@
     second = dest[0] * fold + y
     leads = sorted({orders[i][0] * fold + o for i in range(n_z) for o in range(fold)})
 
-    def make_one_of(place):
+    def make_one_of(place, at=slice(None)):
         for j in leads:
             @pl.when(place == j)
             def _():
-                make_term(j)
+                make_term(j, at)
 
     def line_copy(d, h, up):
-        buf, ss, rs = (got_r, r_ss, r_rs) if up else (got_l, l_ss, l_rs)
+        slot = d + 1 if up else d
         to = z + 1 if up else z - 1
         to = jnp.clip(to, 0, n_z - 1)
         return pltpu.make_async_remote_copy(
-            src_ref=term.at[d * fold + y, piece(h), :], dst_ref=buf.at[d, piece(h), :],
-            send_sem=ss.at[d * pieces + h], recv_sem=rs.at[d * pieces + h],
+            src_ref=term.at[d * fold + y, piece(h), :], dst_ref=got_line.at[slot, piece(h), :],
+            send_sem=line_ss, recv_sem=line_rs.at[slot * pieces + h],
             device_id=(to * fold + y, t), device_id_type=MESH,
         )
 
-    def add_into(d, h, buf):
+    def add_into(d, h, buf, slot):
         own = d * fold + y
-        term[own, piece(h), :] = term[own, piece(h), :] + buf[d, piece(h), :]
+        term[own, piece(h), :] = term[own, piece(h), :] + buf[slot, piece(h), :]
+
+    def line_take(d, h, up):
+        line_copy(d, h, up).wait_recv()
+        add_into(d, h, got_line, d + 1 if up else d)
 
     def hop(k, h):
         d = dest[k]
         y_copies[k][h].wait_recv()
-        add_into(d, h, got_y)
+        add_into(d, h, got_y, d)
 
         @pl.when(d > z)
         def _():
             @pl.when(z > 0)
             def _():
-                line_copy(d, h, True).wait_recv()
-                add_into(d, h, got_r)
+                line_take(d, h, True)
 
             line_copy(d, h, True).start()
 
@@ -230,24 +259,22 @@
         def _():
             @pl.when(z < n_z - 1)
             def _():
-                line_copy(d, h, False).wait_recv()
-                add_into(d, h, got_l)
+                line_take(d, h, False)
 
             line_copy(d, h, False).start()
 
     def low_copy(d, up):
-        buf, ss, rs = (low_r, lr_ss, lr_rs) if up else (low_l, ll_ss, ll_rs)
+        slot = d + 1 if up else d
         to = jnp.clip(z + 1 if up else z - 1, 0, n_z - 1)
         return pltpu.make_async_remote_copy(
-            src_ref=term.at[pl.ds(d * fold, fold), pl.ds(top, low), :], dst_ref=buf.at[d],
-            send_sem=ss.at[d], recv_sem=rs.at[d], device_id=(to * fold + y, t), device_id_type=MESH,
+            src_ref=term.at[pl.ds(d * fold, fold), pl.ds(top, low), :], dst_ref=low_in.at[slot],
+            send_sem=low_ss, recv_sem=low_rs.at[slot], device_id=(to * fold + y, t), device_id_type=MESH,
         )
 
     def low_take(d, up):
         low_copy(d, up).wait_recv()
-        buf = low_r if up else low_l
         at = pl.ds(d * fold, fold)
-        term[at, pl.ds(top, low), :] = term[at, pl.ds(top, low), :] + buf[d]
+        term[at, pl.ds(top, low), :] = term[at, pl.ds(top, low), :] + low_in[d + 1 if up else d]
 
     def low_hop(k):
         d = dest[k]
@@ -284,13 +311,30 @@
 
         low_swap.start()
 
-    make_one_of(lead)
-    y_start(0)
-    make_one_of(second)
+    def activate(at):
+        c = conv[at, :].astype(f32)
+        gains = jnp.concatenate([gain_c[at, :]] * n_blk, axis=1)
+        normed = (c - cols[0:1, :]) * cols[1:2, :] * gains
+        act_t[at, :] = (normed * jax.nn.sigmoid(normed)).astype(jnp.bfloat16)
+
+    def lead_piece(h):
+        at = slice(firsts[h], firsts[h] + sizes[h])
+        activate(at)
+        make_one_of(lead, at)
+        y_copies[0][h].start()
+
+    lead_piece(0)
+    activate(slice(top, None))
+    make_one_of(lead, slice(top, None))
+    make_one_of(second, slice(top, None))
 
     @pl.when(end)
     def _():
         low_hop(0)
+
+    for h in range(1, pieces):
+        lead_piece(h)
+    make_one_of(second, slice(0, top))
 
     for j in range(n_sp):
         if j in leads:
@@ -316,9 +360,9 @@
         d_act[:, at] = d_hat
         put_sums(mom, i, d_hat, d_hat * centered)
 
-    mom_copies = tp_copies(mom, mom_in, mom_ss, mom_rs)
-    for c in mom_copies:
+    for c in tp_copies(mom, mom_in, mom_ss, mom_rs):
         c.start()
+    loads[6].wait()
     for k in range(n_taps):
         taps_b[k] = jnp.broadcast_to(taps[k:k + 1, :].astype(f32), (8, ch))
     grad_acc[...] = jnp.zeros_like(grad_acc)
@@ -330,8 +374,7 @@
         at = pl.ds(pl.multiple_of(i * blk, blk), blk)
         gated_s[at, :] = (pv[:, at].astype(f32) * jax.nn.sigmoid(pg[:, at].astype(f32))).T
 
-    for c in mom_copies:
-        c.wait()
+    tp_wait(mom_in, mom_ss, mom_rs)
     total = mom[...]
     for i in range(n_tp - 1):
         total = total + mom_in[i]
@@ -340,6 +383,12 @@
         cols2[0:1, i * blk:(i + 1) * blk] = total[i:i + 1]
         cols2[1:2, i * blk:(i + 1) * blk] = total[n_blk + i:n_blk + i + 1]
 
+    edge_sums[...] = jnp.zeros_like(edge_sums)
+    edge_sums[0:2, :] = cols[0:2, :blk]
+    edge_sums[2:4, :] = cols2[0:2, :blk]
+    edge_send(2)
+    y_start(1)
+
     @pl.loop(0, n_blk)
     def _(i):
         at = pl.ds(pl.multiple_of(i * blk, blk), blk)
@@ -347,19 +396,6 @@
         inv_std = cols[1:2, at]
         centered = (c - cols[0:1, at]) * inv_std
         ext[at, :] = (inv_std * (d_act[:, at] - cols2[0:1, at] - centered * cols2[1:2, at])).T
-
-    reach = 32
-    back = jnp.maximum(s - 1, 0)
-    halo = pltpu.make_async_remote_copy(
-        src_ref=ext.at[pl.ds(0, reach), :], dst_ref=ext.at[pl.ds(rows, reach), :],
-        send_sem=halo_ss, recv_sem=halo_rs, device_id=(back, t), device_id_type=MESH,
-    )
-
-    @pl.when(s > 0)
-    def _():
-        halo.start()
-
-    y_start(1)
 
     def shift_block(i):
         start = pl.multiple_of(i * reach, reach)
@@ -418,7 +454,16 @@
 
     @pl.when(s < n_sp - 1)
     def _():
-        halo.wait_recv()
+        for i in range(3):
+            edge_copy(i).wait_recv()
+        per_token = edge_sums_in[...].T[:reach]
+        mean_e, inv_e, first_e, second_e = [per_token[:, i:i + 1] for i in range(4)]
+        gain_e = gain[...].astype(f32).reshape(1, ch)
+        centered = (edge_in[0] - mean_e) * inv_e
+        normed = centered * gain_e
+        gate = jax.nn.sigmoid(normed)
+        d_hat = edge_in[1] * gate * (1.0 + normed * (1.0 - gate)) * gain_e
+        ext[pl.ds(rows, reach), :] = inv_e * (d_hat - first_e - centered * second_e)
 
     @pl.when(s == n_sp - 1)
     def _():
@@ -540,57 +585,48 @@
             for h in range(pieces):
                 hop(k, h)
 
+    @pl.when(z < n_z - 1)
+    def _():
+        taps_copy(g_own, True).wait_send()
+
+    @pl.when(z > 0)
+    def _():
+        taps_copy(g_own, False).wait_send()
+
+    @pl.when(s > 0)
+    def _():
+        for i in range(3):
+            edge_copy(i).wait_send()
+
     own = z * fold + y
     low_swap.wait()
     out_w[top:, :] = (term[own, top:, :] + low_y[...]) * scale
     for h in range(pieces):
         y_copies[n_z - 1][h].wait_recv()
-        add_into(z, h, got_y)
+        add_into(z, h, got_y, z)
 
         @pl.when(z > 0)
         def _():
-            line_copy(z, h, True).wait_recv()
-            add_into(z, h, got_r)
+            line_take(z, h, True)
 
         @pl.when(z < n_z - 1)
         def _():
-            line_copy(z, h, False).wait_recv()
-            add_into(z, h, got_l)
+            line_take(z, h, False)
 
         out_w[piece(h), :] = term[own, piece(h), :] * scale
 
     gy.wait()
     out_t[...] = ((g_mid[...] + g_yin[...]) * scale)[:n_taps]
-    for k in range(n_z):
-        for h in range(pieces):
-            y_copies[k][h].wait_send()
-
-    @pl.when(z < n_z - 1)
-    def _():
-        taps_copy(g_own, True).wait_send()
-
-    @pl.when(z > 0)
-    def _():
-        taps_copy(g_own, False).wait_send()
-
-    @pl.when(s > 0)
-    def _():
-        halo.wait_send()
-
-    for k in range(n_z - 1):
-        d = dest[k]
-
-        @pl.when(d > z)
-        def _():
-            for h in range(pieces):
-                line_copy(d, h, True).wait_send()
-            low_copy(d, True).wait_send()
-
-        @pl.when(d < z)
-        def _():
-            for h in range(pieces):
-                line_copy(d, h, False).wait_send()
-            low_copy(d, False).wait_send()
+
+    def all_sent(buf, ss, spare):
+        pltpu.make_async_remote_copy(
+            src_ref=buf, dst_ref=buf, send_sem=ss, recv_sem=spare,
+            device_id=(z * fold + other_y, t), device_id_type=MESH,
+        ).wait_send()
+
+    all_sent(low_in.at[pl.ds(0, n_z - 1)], low_ss, ly_rs)
+    all_sent(got_y, y_ss, ly_rs)
+    all_sent(got_line.at[pl.ds(0, n_z - 1)], line_ss, ly_rs)
 
 
 def fused(n_sp, n_tp, proj_value, proj_gate, conv_saved, conv_taps, norm_gain, out_weight, cotangent):
@@ -600,7 +636,7 @@
     ch = conv_saved.shape[1]
     n_taps = conv_taps.shape[0]
     part = width // n_sp
-    top, low = split_rows(ch)
+    _, top, low = split_rows(ch)
     sums = -(-2 * (rows // 128) // 8) * 8
     dma = pltpu.SemaphoreType.DMA
     V = pltpu.VMEM
@@ -610,23 +646,22 @@
     grad_value, grad_gate, grad_weight, grad_taps = pl.pallas_call(
         functools.partial(kernel, n_sp, n_tp, fold),
         out_shape=(V((ch, rows), bf), V((ch, rows), bf), V((ch, part), f32), V((n_taps, ch), f32)),
-        in_specs=[hb, hb, vm, vm, vm, hb, hb],
+        in_specs=[hb] * 7,
         out_specs=[vm] * 4,
         scratch_shapes=[
-            V((ch, rows), bf), V((ch, rows), bf), V((ch, width), bf), V((width, rows), bf), dma((4,)),
+            V((ch, rows), bf), V((n_taps, ch), bf), V((ch,), bf),
+            V((ch, rows), bf), V((ch, rows), bf), V((ch, width), bf), V((width, rows), bf), dma((7,)),
             V((ch, 128), f32), V((rows, ch), f32), V((rows, ch), f32),
             V((ch, rows), bf), V((ch, rows), f32), V((rows + 32, ch), f32), V((8, rows + 32, ch), f32),
             V((8, rows), f32), V((8, rows), f32),
-            V((n_sp, ch, part), f32), V((n_z, top, part), f32), V((n_z, top, part), f32),
-            V((n_z, top, part), f32),
-            V((n_z, fold, low, part), f32), V((n_z, fold, low, part), f32), V((low, part), f32),
+            V((n_sp, ch, part), f32), V((n_z, top, part), f32), V((n_z + 1, top, part), f32),
+            V((n_z + 1, fold, low, part), f32), V((low, part), f32),
             V((sums, 128), f32), V((n_tp - 1, sums, 128), f32),
             V((sums, 128), f32), V((n_tp - 1, sums, 128), f32),
             V((n_taps, 8, ch), f32), *[V((32, ch), f32)] * 7, V((n_taps, 8, ch), f32),
-            dma((n_tp - 1,)), dma((n_tp - 1,)), dma((n_tp - 1,)), dma((n_tp - 1,)),
-            *[dma((pieces * n_z,))] * 6,
-            dma((n_z,)), dma((n_z,)), dma((n_z,)), dma((n_z,)), dma, dma,
-            *[dma] * 8,
+            V((2, 32, ch), f32), V((2, 32, ch), f32), V((8, 128), f32), V((8, 128), f32),
+            dma, dma, dma, dma, dma, dma((pieces * n_z,)), dma, dma((pieces * (n_z + 1),)),
+            dma, dma((n_z + 1,)), dma, dma, dma((3,)), dma((3,)), *[dma] * 6,
         ],
         compiler_params=pltpu.CompilerParams(
             collective_id=0, has_side_effects=True, vmem_limit_bytes=56 * 1024 * 1024

time: 54.9 us -> 52.1 us (0.949)
  Pallas kernels: 54.1 us -> 51.3 us
    pallas_call x1, Pallas kernels: 53 us -> 50.1 us  [fused(): pl.pallas_call(functools.partial(kernel, n_sp, n_tp, fold), out_shape=(V(...]
where the time goes in v2:
time: 52.1 us; the launch traced here: 51.9 us
  Pallas kernels  51.3 us (98%)
  between operations  0.64 us (1%)
    pallas_call x1, Pallas kernels, fused(): pl.pallas_call(functools.partial(kernel, n_sp, n_tp, fold), out_shape=(V(...  50.1 us
    pallas_call x1, Pallas kernels, fused(): pl.pallas_call(finish, out_shape=tuple((jax.ShapeDtypeStruct(r.shape, r.d...  1.18 us

profile of v2, /device:TPU:0, one launch (start us, length us, event | category | flops | bytes accessed | tf_op | source)
XLA Modules:
  0.0 51.9 jit_solution(16283067939651324679)
XLA Ops:
  0.6 50.1 %shard_map.102 = (bf16[504,512]{1,0:T(8,128)(2,1)S(1)}, bf16[504,512]{1,0:T(8,128)(2,1)S(1)}, f32[504,252]{1,0:T(8,128)S(1)}, f32[31,504]{1,0:T(8,128)S(1)}) custom-call(bf16[504,512]{1,0:T(8,128)(2,1)} %bitcast.7, bf16[504,512]{1,0:T(8,128)(2,1)} %bitcast.8, bf16[504,512]{1,0:T(8,128)(2,1)} %bitcast.9, bf16[31,504]{1,0:T(8,128)(2,1)} %taps_h.1, ...), custom_call_target="tpu_custom_call" | custom-call | tf_op jit(solution)/shard_map/pallas_call | solution.py:646
  50.7 1.2 %shard_map.103 = (bf16[504,512]{1,0:T(8,128)(2,1)}, bf16[504,512]{1,0:T(8,128)(2,1)}, f32[504,252]{1,0:T(8,128)}, f32[31,504]{1,0:T(8,128)}) custom-call(bf16[504,512]{1,0:T(8,128)(2,1)S(1)} %get-tuple-element.12.v_in, bf16[504,512]{1,0:T(8,128)(2,1)S(1)} %get-tuple-element.13.g_in, f32[504,252]{1,0:T(8,128)S(1)} %get-tuple-element.14.w_in, ...), custom_call_target="tpu_custom_call" | custom-call | tf_op jit(solution)/shard_map/pallas_call | solution.py:674

commit v3 on v2

--- a/solution.py
+++ b/solution.py
@@ -47,11 +47,11 @@
 def kernel(
     n_sp, n_tp, fold, pv_h, pg_h, conv_h, taps_h, gain_h, weight_h, cot_h,
     out_v, out_g, out_w, out_t,
-    conv, taps, gain, pv, pg, weight, cot, in_sems, gain_c, gated_s, d_glu_s, act_t, d_act, ext, shifted, cols, cols2, term, got_y, got_line, low_in, low_y,
-    stat, stat_in, mom, mom_in, grad_acc, g_own, g_mid, g_up, g_dn, g_up_out, g_dn_out, g_yin, taps_b, edge_out, edge_in, edge_sums, edge_sums_in,
+    conv, taps, gain, pv, pg, weight, cot, in_sems, conv_sems, cot_sems, ready, gain_c, gated_s, d_glu_s, act_t, d_act, ext, shifted, cols, cols2, term, got_y, got_line, low_in, low_y,
+    stat, stat_in, mom, mom_in, grad_acc, g_own, g_mid, g_up, g_dn, g_up_out, g_dn_out, g_yin, g_total, taps_b, edge_out, edge_in, edge_sums, edge_sums_in,
     stat_ss, stat_rs, mom_ss, mom_rs, y_ss, y_rs, line_ss, line_rs,
     low_ss, low_rs, ly_ss, ly_rs, edge_ss, edge_rs,
-    gu_ss, gu_rs, gd_ss, gd_rs, gy_ss, gy_rs,
+    gu_ss, gu_rs, gd_ss, gd_rs, gy_ss, gy_rs, gt_ss, gt_rs,
 ):
     s = lax.axis_index("sp")
     t = lax.axis_index("tp")
@@ -73,10 +73,17 @@
     loads = [
         pltpu.make_async_copy(a, b, in_sems.at[i])
         for i, (a, b) in enumerate([
-            (cot_h, cot), (weight_h, weight), (pv_h, pv), (pg_h, pg), (conv_h, conv), (gain_h, gain), (taps_h, taps)
+            (weight_h, weight), (pv_h, pv), (pg_h, pg), (gain_h, gain), (taps_h, taps)
         ])
     ]
-    loads[4].start()
+    conv_loads = [
+        pltpu.make_async_copy(
+            conv_h.at[:, pl.ds(i * blk, blk)], conv.at[:, pl.ds(i * blk, blk)], conv_sems.at[i]
+        )
+        for i in range(n_blk)
+    ]
+    for c in conv_loads:
+        c.start()
 
     barrier = pltpu.get_barrier_semaphore()
 
@@ -85,15 +92,10 @@
 
     for i in range(1, n_tp):
         greet(s, lax.rem(t + i, n_tp))
-    greet(z * fold + other_y, t)
-
-    @pl.when(z > 0)
-    def _():
-        greet(s - fold, t)
-
-        @pl.when(y == 0)
-        def _():
-            greet(s - 1, t)
+
+    @pl.when(y < fold - 1)
+    def _():
+        greet(s + 1, t)
 
     @pl.when(z < n_z - 1)
     def _():
@@ -103,8 +105,17 @@
         def _():
             greet(s + 1, t)
 
-    for i in (0, 1, 5, 2, 3, 6):
-        loads[i].start()
+    wide_blk = 256 if rows % 256 == 0 else 128
+    cot_loads = [
+        pltpu.make_async_copy(
+            cot_h.at[:, pl.ds(i, wide_blk)], cot.at[:, pl.ds(i, wide_blk)], cot_sems.at[i // wide_blk]
+        )
+        for i in range(0, rows, wide_blk)
+    ]
+    loads[3].start()
+    loads[0].start()
+    for c in cot_loads:
+        c.start()
 
     def put_sums(ref, i, first, second):
         ref[pl.ds(i, 1), :] = jnp.sum(first, axis=0, keepdims=True)
@@ -114,17 +125,22 @@
         stat[...] = jnp.zeros_like(stat)
         mom[...] = jnp.zeros_like(mom)
 
-    loads[4].wait()
-
-    @pl.loop(0, n_blk)
-    def _(i):
-        at = pl.ds(pl.multiple_of(i * blk, blk), blk)
-        c = conv[:, at].astype(f32)
+    for i in range(n_blk):
+        conv_loads[i].wait()
+        c = conv[:, i * blk:(i + 1) * blk].astype(f32)
         put_sums(stat, i, c, c * c)
 
-    below = jnp.where(z > 0, jnp.where(y == 0, 2, 1), 0)
-    above = jnp.where(z < n_z - 1, jnp.where(y == fold - 1, 2, 1), 0)
-    pl.semaphore_wait(barrier, n_tp + below + above)
+    first_in_row = jnp.where(y == 0, 1, 0)
+    below = jnp.where(z > 0, 1 + first_in_row, 0)
+    pl.semaphore_wait(barrier, n_tp - 1 + (1 - first_in_row) + below)
+
+    @pl.when(y > 0)
+    def _():
+        pl.semaphore_signal(ready, inc=1, device_id=(s - 1, t), device_id_type=MESH)
+
+    @pl.when(z > 0)
+    def _():
+        pl.semaphore_signal(ready, inc=1, device_id=(s - fold, t), device_id_type=MESH)
 
     def tp_copies(src, dst, ss, rs):
         return [
@@ -161,21 +177,19 @@
 
     edge_out[0] = conv[:, :blk].astype(f32).T[:reach]
     edge_send(0)
-    loads[5].wait()
+    loads[3].wait()
     gain_c[...] = jnp.broadcast_to(gain[...].astype(f32).reshape(1, ch), (128, ch)).T
     loads[0].wait()
-    loads[1].wait()
-    wide_blk = 256 if rows % 256 == 0 else 128
+    cot_loads[0].wait()
 
     d_act[:, :wide_blk] = jnp.dot(weight[...], cot[:, :wide_blk], preferred_element_type=f32)
     edge_out[1] = d_act[:, :blk].T[:reach]
     edge_send(1)
 
-    @pl.loop(1, rows // wide_blk)
-    def _(i):
-        at = pl.ds(pl.multiple_of(i * wide_blk, wide_blk), wide_blk)
-        d_act[:, at] = jnp.dot(weight[...], cot[:, at], preferred_element_type=f32)
-
+    for i in (1, 2, 4):
+        loads[i].start()
+    for c in cot_loads[1:]:
+        c.wait()
     tp_wait(stat_in, stat_ss, stat_rs)
     total = stat[...]
     for i in range(n_tp - 1):
@@ -323,6 +337,11 @@
         make_one_of(lead, at)
         y_copies[0][h].start()
 
+
+    @pl.when(jnp.logical_or(y == 0, z < n_z - 1))
+    def _():
+        pl.semaphore_wait(ready, first_in_row + jnp.where(z < n_z - 1, 1, 0))
+
     lead_piece(0)
     activate(slice(top, None))
     make_one_of(lead, slice(top, None))
@@ -348,6 +367,11 @@
     def _():
         for k in range(1, n_z - 1):
             low_hop(k)
+
+    @pl.loop(1, rows // wide_blk)
+    def _(i):
+        at = pl.ds(pl.multiple_of(i * wide_blk, wide_blk), wide_blk)
+        d_act[:, at] = jnp.dot(weight[...], cot[:, at], preferred_element_type=f32)
 
     @pl.loop(0, n_blk)
     def _(i):
@@ -362,12 +386,12 @@
 
     for c in tp_copies(mom, mom_in, mom_ss, mom_rs):
         c.start()
-    loads[6].wait()
+    loads[4].wait()
     for k in range(n_taps):
         taps_b[k] = jnp.broadcast_to(taps[k:k + 1, :].astype(f32), (8, ch))
     grad_acc[...] = jnp.zeros_like(grad_acc)
+    loads[1].wait()
     loads[2].wait()
-    loads[3].wait()
 
     @pl.loop(0, n_blk)
     def _(i):
@@ -492,17 +516,18 @@
         src = g_up if up else g_dn
         out = g_up_out if up else g_dn_out
         taps_copy(g_own, up).wait_recv()
-        out[...] = g_own[...] + src[...]
-        taps_copy(out, up).start()
+
+        @pl.when(z < n_z - 2 if up else z > 1)
+        def _():
+            out[...] = g_own[...] + src[...]
+            taps_copy(out, up).start()
 
     @pl.when(z == 0)
     def _():
-        g_up[...] = jnp.zeros_like(g_up)
         taps_copy(g_own, True).start()
 
     @pl.when(z == n_z - 1)
     def _():
-        g_dn[...] = jnp.zeros_like(g_dn)
         taps_copy(g_own, False).start()
 
     y_start(2, 0, pieces if n_z > 3 else 2)
@@ -542,42 +567,44 @@
         hop(0, 3)
 
     low_end()
-    if n_z > 3:
-        y_start(n_z - 1, 0, 2)
-
-    @pl.when(end)
-    def _():
-        for h in range(pieces):
-            hop(n_z - 2, h)
-
-    @pl.when(mid)
-    def _():
-        @pl.when(2 * z < n_z)
-        def _():
-            taps_pass(False)
-
-        @pl.when(2 * z >= n_z)
-        def _():
-            taps_pass(True)
-
-        for h in range(pieces):
-            hop(1, h)
-
-    @pl.when(z == 0)
-    def _():
-        taps_copy(g_own, False).wait_recv()
-
-    @pl.when(z == n_z - 1)
-    def _():
-        taps_copy(g_own, True).wait_recv()
-
-    g_mid[...] = g_own[...] + g_up[...] + g_dn[...]
     gy = pltpu.make_async_remote_copy(
         src_ref=g_mid, dst_ref=g_yin, send_sem=gy_ss, recv_sem=gy_rs,
         device_id=(z * fold + other_y, t), device_id_type=MESH,
     )
-    gy.start()
-    y_start(n_z - 1, 2, pieces)
+
+    def total_copy(up):
+        to = jnp.clip(z + 1 if up else z - 1, 0, n_z - 1)
+        return pltpu.make_async_remote_copy(
+            src_ref=g_total, dst_ref=g_yin, send_sem=gt_ss.at[int(up)], recv_sem=gt_rs,
+            device_id=(to * fold + y, t), device_id_type=MESH,
+        )
+
+    y_start(n_z - 1, 0, 1)
+
+    @pl.when(end)
+    def _():
+        y_start(n_z - 1, 1, pieces)
+
+    @pl.when(end)
+    def _():
+        for h in range(pieces):
+            hop(n_z - 2, h)
+
+    @pl.when(mid)
+    def _():
+        @pl.when(2 * z < n_z)
+        def _():
+            taps_pass(False)
+
+        @pl.when(2 * z >= n_z)
+        def _():
+            taps_pass(True)
+
+        g_mid[...] = g_own[...] + g_up[...] + g_dn[...]
+        gy.start()
+        y_start(n_z - 1, 1, pieces)
+        for h in range(pieces):
+            hop(1, h)
 
     @pl.when(mid)
     def _():
@@ -585,11 +612,11 @@
             for h in range(pieces):
                 hop(k, h)
 
-    @pl.when(z < n_z - 1)
+    @pl.when(z < n_z - 2)
     def _():
         taps_copy(g_own, True).wait_send()
 
-    @pl.when(z > 0)
+    @pl.when(z > 1)
     def _():
         taps_copy(g_own, False).wait_send()
 
@@ -602,6 +629,20 @@
     low_swap.wait()
     out_w[top:, :] = (term[own, top:, :] + low_y[...]) * scale
     for h in range(pieces):
+        if h == 1:
+            @pl.when(mid)
+            def _():
+                gy.wait()
+                g_total[...] = g_mid[...] + g_yin[...]
+
+                @pl.when(z == 1)
+                def _():
+                    total_copy(False).start()
+
+                @pl.when(z == n_z - 2)
+                def _():
+                    total_copy(True).start()
+
         y_copies[n_z - 1][h].wait_recv()
         add_into(z, h, got_y, z)
 
@@ -615,8 +656,23 @@
 
         out_w[piece(h), :] = term[own, piece(h), :] * scale
 
-    gy.wait()
-    out_t[...] = ((g_mid[...] + g_yin[...]) * scale)[:n_taps]
+    @pl.when(end)
+    def _():
+        total_copy(True).wait_recv()
+        out_t[...] = (g_yin[...] * scale)[:n_taps]
+
+    @pl.when(mid)
+    def _():
+        out_t[...] = (g_total[...] * scale)[:n_taps]
+
+        @pl.when(z == 1)
+        def _():
+            total_copy(False).wait_send()
+
+        @pl.when(z == n_z - 2)
+        def _():
+            total_copy(True).wait_send()
+
 
     def all_sent(buf, ss, spare):
         pltpu.make_async_remote_copy(
@@ -650,7 +706,7 @@
         out_specs=[vm] * 4,
         scratch_shapes=[
             V((ch, rows), bf), V((n_taps, ch), bf), V((ch,), bf),
-            V((ch, rows), bf), V((ch, rows), bf), V((ch, width), bf), V((width, rows), bf), dma((7,)),
+            V((ch, rows), bf), V((ch, rows), bf), V((ch, width), bf), V((width, rows), bf), dma((5,)), dma((rows // 128,)), dma((rows // (256 if rows % 256 == 0 else 128),)), pltpu.SemaphoreType.REGULAR,
             V((ch, 128), f32), V((rows, ch), f32), V((rows, ch), f32),
             V((ch, rows), bf), V((ch, rows), f32), V((rows + 32, ch), f32), V((8, rows + 32, ch), f32),
             V((8, rows), f32), V((8, rows), f32),
@@ -658,10 +714,10 @@
             V((n_z + 1, fold, low, part), f32), V((low, part), f32),
             V((sums, 128), f32), V((n_tp - 1, sums, 128), f32),
             V((sums, 128), f32), V((n_tp - 1, sums, 128), f32),
-            V((n_taps, 8, ch), f32), *[V((32, ch), f32)] * 7, V((n_taps, 8, ch), f32),
+            V((n_taps, 8, ch), f32), *[V((32, ch), f32)] * 8, V((n_taps, 8, ch), f32),
             V((2, 32, ch), f32), V((2, 32, ch), f32), V((8, 128), f32), V((8, 128), f32),
             dma, dma, dma, dma, dma, dma((pieces * n_z,)), dma, dma((pieces * (n_z + 1),)),
-            dma, dma((n_z + 1,)), dma, dma, dma((3,)), dma((3,)), *[dma] * 6,
+            dma, dma((n_z + 1,)), dma, dma, dma((3,)), dma((3,)), *[dma] * 6, dma((2,)), dma,
         ],
         compiler_params=pltpu.CompilerParams(
             collective_id=0, has_side_effects=True, vmem_limit_bytes=56 * 1024 * 1024

time: 52.1 us -> 50.5 us (0.969)
  Pallas kernels: 51.3 us -> 49.5 us
    pallas_call x1, Pallas kernels: 50.1 us -> 48.4 us  [fused(): pl.pallas_call(functools.partial(kernel, n_sp, n_tp, fold), out_shape=(V(...]
where the time goes in v3:
time: 50.5 us; the launch traced here: 50.2 us
  Pallas kernels  49.5 us (98%)
  between operations  0.64 us (1%)
    pallas_call x1, Pallas kernels, fused(): pl.pallas_call(functools.partial(kernel, n_sp, n_tp, fold), out_shape=(V(...  48.4 us
    pallas_call x1, Pallas kernels, fused(): pl.pallas_call(finish, out_shape=tuple((jax.ShapeDtypeStruct(r.shape, r.d...  1.18 us

profile of v3, /device:TPU:0, one launch (start us, length us, event | category | flops | bytes accessed | tf_op | source)
XLA Modules:
  0.0 50.2 jit_solution(4732796270286025769)
XLA Ops:
  0.6 48.4 %shard_map.102 = (bf16[504,512]{1,0:T(8,128)(2,1)S(1)}, bf16[504,512]{1,0:T(8,128)(2,1)S(1)}, f32[504,252]{1,0:T(8,128)S(1)}, f32[31,504]{1,0:T(8,128)S(1)}) custom-call(bf16[504,512]{1,0:T(8,128)(2,1)} %bitcast.7, bf16[504,512]{1,0:T(8,128)(2,1)} %bitcast.8, bf16[504,512]{1,0:T(8,128)(2,1)} %bitcast.9, bf16[31,504]{1,0:T(8,128)(2,1)} %taps_h.1, ...), custom_call_target="tpu_custom_call" | custom-call | tf_op jit(solution)/shard_map/pallas_call | solution.py:702
  49.0 1.2 %shard_map.103 = (bf16[504,512]{1,0:T(8,128)(2,1)}, bf16[504,512]{1,0:T(8,128)(2,1)}, f32[504,252]{1,0:T(8,128)}, f32[31,504]{1,0:T(8,128)}) custom-call(bf16[504,512]{1,0:T(8,128)(2,1)S(1)} %get-tuple-element.12.v_in, bf16[504,512]{1,0:T(8,128)(2,1)S(1)} %get-tuple-element.13.g_in, f32[504,252]{1,0:T(8,128)S(1)} %get-tuple-element.14.w_in, ...), custom_call_target="tpu_custom_call" | custom-call | tf_op jit(solution)/shard_map/pallas_call | solution.py:730

commit v4 on v3

--- a/solution.py
+++ b/solution.py
@@ -23,9 +23,10 @@
 
 
 def split_rows(ch):
-    units = ch * 17 // 20 // 8
-    sizes = [8 * (units // pieces + (i < units % pieces)) for i in range(pieces)]
-    return sizes, sum(sizes), ch - sum(sizes)
+    low, wide = ch // 6 // 8 * 8, ch // 9 * 2 // 8 * 8
+    units = (ch - wide) // 8
+    sizes = [8 * (units // (pieces - 1) + (i < units % (pieces - 1))) for i in range(pieces - 1)]
+    return sizes + [wide - low], low, wide
 
 
 def lookup(table, place):
@@ -48,9 +49,9 @@
     n_sp, n_tp, fold, pv_h, pg_h, conv_h, taps_h, gain_h, weight_h, cot_h,
     out_v, out_g, out_w, out_t,
     conv, taps, gain, pv, pg, weight, cot, in_sems, conv_sems, cot_sems, ready, gain_c, gated_s, d_glu_s, act_t, d_act, ext, shifted, cols, cols2, term, got_y, got_line, low_in, low_y,
-    stat, stat_in, mom, mom_in, grad_acc, g_own, g_mid, g_up, g_dn, g_up_out, g_dn_out, g_yin, g_total, taps_b, edge_out, edge_in, edge_sums, edge_sums_in,
+    stat, stat_in, mom, mom_in, grad_acc, g_own, g_mid, g_up, g_dn, g_up_out, g_dn_out, g_yin, g_total, taps_b, edge_out, edge_in, edge_sums, edge_sums_in, wide_in, wide_y,
     stat_ss, stat_rs, mom_ss, mom_rs, y_ss, y_rs, line_ss, line_rs,
-    low_ss, low_rs, ly_ss, ly_rs, edge_ss, edge_rs,
+    low_ss, low_rs, wide_ss, wide_rs, ly_ss, ly_rs, edge_ss, edge_rs,
     gu_ss, gu_rs, gd_ss, gd_rs, gy_ss, gy_rs, gt_ss, gt_rs,
 ):
     s = lax.axis_index("sp")
@@ -66,7 +67,9 @@
     scale = 1.0 / math.sqrt(rows * n_sp)
     blk = 128
     n_blk = rows // blk
-    sizes, top, low = split_rows(ch)
+    sizes, low, wide = split_rows(ch)
+    base, top, swing = ch - wide, ch - low, wide - low
+    last = n_z - 1
     end = jnp.logical_or(z == 0, z == n_z - 1)
     mid = jnp.logical_and(z > 0, z < n_z - 1)
 
@@ -212,15 +215,20 @@
         sem = dest[k] * pieces + h
         return pltpu.make_async_remote_copy(
             src_ref=term.at[dest[k] * fold + other_y, piece(h), :], dst_ref=got_y.at[dest[k], piece(h), :],
-            send_sem=y_ss, recv_sem=y_rs.at[sem],
+            send_sem=y_ss.at[int(h == pieces - 1)], recv_sem=y_rs.at[sem],
             device_id=(z * fold + other_y, t), device_id_type=MESH,
         )
 
     y_copies = [[y_copy(k, h) for h in range(pieces)] for k in range(n_z)]
 
-    def y_start(k, first=0, last=pieces):
-        for h in range(first, last):
-            y_copies[k][h].start()
+    def y_start(k, first=0, past=pieces):
+        for h in range(first, past):
+            if h < pieces - 1:
+                y_copies[k][h].start()
+            else:
+                @pl.when(dest[k] != last)
+                def _():
+                    y_copies[k][h].start()
 
     def make_term(j, at=slice(None)):
         term[j, at, :] = lax.dot_general(
@@ -244,7 +252,7 @@
         to = jnp.clip(to, 0, n_z - 1)
         return pltpu.make_async_remote_copy(
             src_ref=term.at[d * fold + y, piece(h), :], dst_ref=got_line.at[slot, piece(h), :],
-            send_sem=line_ss, recv_sem=line_rs.at[slot * pieces + h],
+            send_sem=line_ss.at[int(h == pieces - 1)], recv_sem=line_rs.at[slot * pieces + h],
             device_id=(to * fold + y, t), device_id_type=MESH,
         )
 
@@ -256,7 +264,7 @@
         line_copy(d, h, up).wait_recv()
         add_into(d, h, got_line, d + 1 if up else d)
 
-    def hop(k, h):
+    def hop_always(k, h):
         d = dest[k]
         y_copies[k][h].wait_recv()
         add_into(d, h, got_y, d)
@@ -276,6 +284,14 @@
                 line_take(d, h, False)
 
             line_copy(d, h, False).start()
+
+    def hop(k, h):
+        if h < pieces - 1:
+            hop_always(k, h)
+        else:
+            @pl.when(dest[k] != last)
+            def _():
+                hop_always(k, h)
 
     def low_copy(d, up):
         slot = d + 1 if up else d
@@ -290,10 +306,29 @@
         at = pl.ds(d * fold, fold)
         term[at, pl.ds(top, low), :] = term[at, pl.ds(top, low), :] + low_in[d + 1 if up else d]
 
+    wide_copy = pltpu.make_async_remote_copy(
+        src_ref=term.at[pl.ds(last * fold, fold), pl.ds(base, wide), :], dst_ref=wide_in,
+        send_sem=wide_ss, recv_sem=wide_rs,
+        device_id=(jnp.clip(z + 1, 0, last) * fold + y, t), device_id_type=MESH,
+    )
+
+    def wide_take():
+        wide_copy.wait_recv()
+        at = slice(last * fold, n_sp)
+        term[at, base:, :] = term[at, base:, :] + wide_in[...]
+
     def low_hop(k):
         d = dest[k]
 
-        @pl.when(d > z)
+        @pl.when(d == last)
+        def _():
+            @pl.when(z > 0)
+            def _():
+                wide_take()
+
+            wide_copy.start()
+
+        @pl.when(jnp.logical_and(d > z, d < last))
         def _():
             @pl.when(z > 0)
             def _():
@@ -303,27 +338,32 @@
 
         @pl.when(d < z)
         def _():
-            @pl.when(z < n_z - 1)
+            @pl.when(z < last)
             def _():
                 low_take(d, False)
 
             low_copy(d, False).start()
 
-    low_swap = pltpu.make_async_remote_copy(
-        src_ref=term.at[z * fold + other_y, pl.ds(top, low), :], dst_ref=low_y,
-        send_sem=ly_ss, recv_sem=ly_rs, device_id=(z * fold + other_y, t), device_id_type=MESH,
-    )
+    def swap_copy(first, count, into):
+        return pltpu.make_async_remote_copy(
+            src_ref=term.at[z * fold + other_y, pl.ds(first, count), :], dst_ref=into,
+            send_sem=ly_ss, recv_sem=ly_rs, device_id=(z * fold + other_y, t), device_id_type=MESH,
+        )
 
     def low_end():
-        @pl.when(z > 0)
-        def _():
-            low_take(z, True)
-
-        @pl.when(z < n_z - 1)
-        def _():
+        @pl.when(z < last)
+        def _():
+            @pl.when(z > 0)
+            def _():
+                low_take(z, True)
+
             low_take(z, False)
-
-        low_swap.start()
+            swap_copy(top, low, low_y).start()
+
+        @pl.when(z == last)
+        def _():
+            wide_take()
+            swap_copy(base, wide, wide_y).start()
 
     def activate(at):
         c = conv[at, :].astype(f32)
@@ -335,25 +375,33 @@
         at = slice(firsts[h], firsts[h] + sizes[h])
         activate(at)
         make_one_of(lead, at)
-        y_copies[0][h].start()
+        y_start(0, h, h + 1)
 
 
     @pl.when(jnp.logical_or(y == 0, z < n_z - 1))
     def _():
         pl.semaphore_wait(ready, first_in_row + jnp.where(z < n_z - 1, 1, 0))
 
-    lead_piece(0)
-    activate(slice(top, None))
-    make_one_of(lead, slice(top, None))
-    make_one_of(second, slice(top, None))
+    @pl.when(z < n_z - 1)
+    def _():
+        lead_piece(0)
+
+    activate(slice(base, None))
+    make_one_of(lead, slice(base, None))
+    make_one_of(second, slice(base, None))
 
     @pl.when(end)
     def _():
         low_hop(0)
 
-    for h in range(1, pieces):
+    @pl.when(z == n_z - 1)
+    def _():
+        lead_piece(0)
+
+    for h in range(1, pieces - 1):
         lead_piece(h)
-    make_one_of(second, slice(0, top))
+    y_start(0, pieces - 1)
+    make_one_of(second, slice(0, base))
 
     for j in range(n_sp):
         if j in leads:
@@ -603,14 +651,10 @@
         g_mid[...] = g_own[...] + g_up[...] + g_dn[...]
         gy.start()
         y_start(n_z - 1, 1, pieces)
-        for h in range(pieces):
-            hop(1, h)
-
-    @pl.when(mid)
-    def _():
-        for k in range(2, n_z - 1):
-            for h in range(pieces):
-                hop(k, h)
+        later = [(k, h) for k in range(1, n_z - 1) for h in range(pieces)]
+        for k, h in sorted(later, key=lambda p: (p[1] + 2 * p[0], p[0])):
+            hop(k, h)
+
 
     @pl.when(z < n_z - 2)
     def _():
@@ -626,35 +670,50 @@
             edge_copy(i).wait_send()
 
     own = z * fold + y
-    low_swap.wait()
-    out_w[top:, :] = (term[own, top:, :] + low_y[...]) * scale
-    for h in range(pieces):
-        if h == 1:
-            @pl.when(mid)
-            def _():
-                gy.wait()
-                g_total[...] = g_mid[...] + g_yin[...]
-
-                @pl.when(z == 1)
-                def _():
-                    total_copy(False).start()
-
-                @pl.when(z == n_z - 2)
-                def _():
-                    total_copy(True).start()
-
-        y_copies[n_z - 1][h].wait_recv()
+
+    @pl.when(z < last)
+    def _():
+        swap_copy(top, low, low_y).wait()
+        out_w[top:, :] = (term[own, top:, :] + low_y[...]) * scale
+
+    @pl.when(z == last)
+    def _():
+        swap_copy(base, wide, wide_y).wait()
+        out_w[base:, :] = (term[own, base:, :] + wide_y[...]) * scale
+
+    def own_piece(h):
+        y_copies[last][h].wait_recv()
         add_into(z, h, got_y, z)
 
         @pl.when(z > 0)
         def _():
             line_take(z, h, True)
 
-        @pl.when(z < n_z - 1)
+        @pl.when(z < last)
         def _():
             line_take(z, h, False)
 
         out_w[piece(h), :] = term[own, piece(h), :] * scale
+
+    @pl.when(mid)
+    def _():
+        gy.wait()
+        g_total[...] = g_mid[...] + g_yin[...]
+
+        @pl.when(z == 1)
+        def _():
+            total_copy(False).start()
+
+        @pl.when(z == n_z - 2)
+        def _():
+            total_copy(True).start()
+
+    for h in range(pieces - 1):
+        own_piece(h)
+
+    @pl.when(z < last)
+    def _():
+        own_piece(pieces - 1)
 
     @pl.when(end)
     def _():
@@ -680,9 +739,22 @@
             device_id=(z * fold + other_y, t), device_id_type=MESH,
         ).wait_send()
 
-    all_sent(low_in.at[pl.ds(0, n_z - 1)], low_ss, ly_rs)
-    all_sent(got_y, y_ss, ly_rs)
-    all_sent(got_line.at[pl.ds(0, n_z - 1)], line_ss, ly_rs)
+    all_sent(got_y.at[:, pl.ds(0, base), :], y_ss.at[0], ly_rs)
+    all_sent(got_y.at[pl.ds(0, last), pl.ds(base, swing), :], y_ss.at[1], ly_rs)
+    all_sent(got_line.at[pl.ds(0, last), pl.ds(0, base), :], line_ss.at[0], ly_rs)
+
+    def by_place(count):
+        all_sent(low_in.at[pl.ds(0, count)], low_ss, ly_rs)
+        all_sent(got_line.at[pl.ds(0, count), pl.ds(base, swing), :], line_ss.at[1], ly_rs)
+
+    @pl.when(z < last)
+    def _():
+        wide_copy.wait_send()
+        by_place(last - 1)
+
+    @pl.when(z == last)
+    def _():
+        by_place(last)
 
 
 def fused(n_sp, n_tp, proj_value, proj_gate, conv_saved, conv_taps, norm_gain, out_weight, cotangent):
@@ -692,7 +764,8 @@
     ch = conv_saved.shape[1]
     n_taps = conv_taps.shape[0]
     part = width // n_sp
-    _, top, low = split_rows(ch)
+    _, low, wide = split_rows(ch)
+    top = ch - low
     sums = -(-2 * (rows // 128) // 8) * 8
     dma = pltpu.SemaphoreType.DMA
     V = pltpu.VMEM
@@ -715,9 +788,9 @@
             V((sums, 128), f32), V((n_tp - 1, sums, 128), f32),
             V((sums, 128), f32), V((n_tp - 1, sums, 128), f32),
             V((n_taps, 8, ch), f32), *[V((32, ch), f32)] * 8, V((n_taps, 8, ch), f32),
-            V((2, 32, ch), f32), V((2, 32, ch), f32), V((8, 128), f32), V((8, 128), f32),
-            dma, dma, dma, dma, dma, dma((pieces * n_z,)), dma, dma((pieces * (n_z + 1),)),
-            dma, dma((n_z + 1,)), dma, dma, dma((3,)), dma((3,)), *[dma] * 6, dma((2,)), dma,
+            V((2, 32, ch), f32), V((2, 32, ch), f32), V((8, 128), f32), V((8, 128), f32), V((fold, wide, part), f32), V((wide, part), f32),
+            dma, dma, dma, dma, dma((2,)), dma((pieces * n_z,)), dma((2,)), dma((pieces * (n_z + 1),)),
+            dma, dma((n_z + 1,)), dma, dma, dma, dma, dma((3,)), dma((3,)), *[dma] * 6, dma((2,)), dma,
         ],
         compiler_params=pltpu.CompilerParams(
             collective_id=0, has_side_effects=True, vmem_limit_bytes=56 * 1024 * 1024

time: 50.5 us -> 50.4 us (level)
  no operation moved by 1% of the time
where the time goes in v4:
time: 50.4 us; the launch traced here: 50.2 us
  Pallas kernels  49.6 us (98%)
  between operations  0.64 us (1%)
    pallas_call x1, Pallas kernels, fused(): pl.pallas_call(functools.partial(kernel, n_sp, n_tp, fold), out_shape=(V(...  48.4 us
    pallas_call x1, Pallas kernels, fused(): pl.pallas_call(finish, out_shape=tuple((jax.ShapeDtypeStruct(r.shape, r.d...  1.18 us

profile of v4, /device:TPU:0, one launch (start us, length us, event | category | flops | bytes accessed | tf_op | source)
XLA Modules:
  0.0 50.2 jit_solution(16274991299864037324)
XLA Ops:
  0.6 48.4 %shard_map.102 = (bf16[504,512]{1,0:T(8,128)(2,1)S(1)}, bf16[504,512]{1,0:T(8,128)(2,1)S(1)}, f32[504,252]{1,0:T(8,128)S(1)}, f32[31,504]{1,0:T(8,128)S(1)}) custom-call(bf16[504,512]{1,0:T(8,128)(2,1)} %bitcast.7, bf16[504,512]{1,0:T(8,128)(2,1)} %bitcast.8, bf16[504,512]{1,0:T(8,128)(2,1)} %bitcast.9, bf16[31,504]{1,0:T(8,128)(2,1)} %taps_h.1, ...), custom_call_target="tpu_custom_call" | custom-call | tf_op jit(solution)/shard_map/pallas_call | solution.py:775
  49.1 1.2 %shard_map.103 = (bf16[504,512]{1,0:T(8,128)(2,1)}, bf16[504,512]{1,0:T(8,128)(2,1)}, f32[504,252]{1,0:T(8,128)}, f32[31,504]{1,0:T(8,128)}) custom-call(bf16[504,512]{1,0:T(8,128)(2,1)S(1)} %get-tuple-element.12.v_in, bf16[504,512]{1,0:T(8,128)(2,1)S(1)} %get-tuple-element.13.g_in, f32[504,252]{1,0:T(8,128)S(1)} %get-tuple-element.14.w_in, ...), custom_call_target="tpu_custom_call" | custom-call | tf_op jit(solution)/shard_map/pallas_call | solution.py:803

commit v5 on v4

--- a/solution.py
+++ b/solution.py
@@ -23,7 +23,7 @@
 
 
 def split_rows(ch):
-    low, wide = ch // 6 // 8 * 8, ch // 9 * 2 // 8 * 8
+    low, wide = ch // 6 // 8 * 8, ch // 21 * 5 // 8 * 8
     units = (ch - wide) // 8
     sizes = [8 * (units // (pieces - 1) + (i < units % (pieces - 1))) for i in range(pieces - 1)]
     return sizes + [wide - low], low, wide
@@ -382,7 +382,7 @@
     def _():
         pl.semaphore_wait(ready, first_in_row + jnp.where(z < n_z - 1, 1, 0))
 
-    @pl.when(z < n_z - 1)
+    @pl.when(mid)
     def _():
         lead_piece(0)
 
@@ -394,7 +394,7 @@
     def _():
         low_hop(0)
 
-    @pl.when(z == n_z - 1)
+    @pl.when(end)
     def _():
         lead_piece(0)
 

time: 50.4 us -> 50.3 us (level)
  no operation moved by 1% of the time
where the time goes in v5:
time: 50.3 us; the launch traced here: 50.1 us
  Pallas kernels  49.5 us (98%)
  between operations  0.64 us (1%)
    pallas_call x1, Pallas kernels, fused(): pl.pallas_call(functools.partial(kernel, n_sp, n_tp, fold), out_shape=(V(...  48.3 us
    pallas_call x1, Pallas kernels, fused(): pl.pallas_call(finish, out_shape=tuple((jax.ShapeDtypeStruct(r.shape, r.d...  1.18 us

profile of v5, /device:TPU:0, one launch (start us, length us, event | category | flops | bytes accessed | tf_op | source)
XLA Modules:
  0.0 50.1 jit_solution(11574960227180233685)
XLA Ops:
  0.6 48.3 %shard_map.102 = (bf16[504,512]{1,0:T(8,128)(2,1)S(1)}, bf16[504,512]{1,0:T(8,128)(2,1)S(1)}, f32[504,252]{1,0:T(8,128)S(1)}, f32[31,504]{1,0:T(8,128)S(1)}) custom-call(bf16[504,512]{1,0:T(8,128)(2,1)} %bitcast.7, bf16[504,512]{1,0:T(8,128)(2,1)} %bitcast.8, bf16[504,512]{1,0:T(8,128)(2,1)} %bitcast.9, bf16[31,504]{1,0:T(8,128)(2,1)} %taps_h.1, ...), custom_call_target="tpu_custom_call" | custom-call | tf_op jit(solution)/shard_map/pallas_call | solution.py:775
  48.9 1.2 %shard_map.103 = (bf16[504,512]{1,0:T(8,128)(2,1)}, bf16[504,512]{1,0:T(8,128)(2,1)}, f32[504,252]{1,0:T(8,128)}, f32[31,504]{1,0:T(8,128)}) custom-call(bf16[504,512]{1,0:T(8,128)(2,1)S(1)} %get-tuple-element.12.v_in, bf16[504,512]{1,0:T(8,128)(2,1)S(1)} %get-tuple-element.13.g_in, f32[504,252]{1,0:T(8,128)S(1)} %get-tuple-element.14.w_in, ...), custom_call_target="tpu_custom_call" | custom-call | tf_op jit(solution)/shard_map/pallas_call | solution.py:803
